TPU v7x, 32 devices: a whole 2x2x4 slice. The times are simulated.
32 devices in a mesh: grp: 2 (over y), st: 4 (over z), tp: 4 (over x, core).
Axes of the slice: x: 2, y: 2, z: 4, core: 2. Of those that a mesh axis runs over, the one named last changes fastest.
Arguments:
- pass_ids: int32 [64, 4], P(('grp', 'st')), parts along dimension 0, may hold values from 0 to 63, as said below
- store: bfloat16 [64, 64, 2048], P('st', None, 'tp'), may hold values from -6 to 6
- queries: bfloat16 [8192, 1024], P(('grp', 'st'), 'tp'), parts along dimension 0, may hold values from -40 to 40
- gate_pre: bfloat16 [8192, 1024], P(('grp', 'st'), 'tp'), parts along dimension 0, may hold values from -6 to 6
- w_query: bfloat16 [2048, 1024], P(None, 'tp'), may hold values from -0.125 to 0.125
- w_gate: bfloat16 [2048, 1024], P(None, 'tp'), may hold values from -0.125 to 0.125
- w_key: bfloat16 [2048, 1024], P(None, 'tp'), may hold values from -0.125 to 0.125
- w_value: bfloat16 [2048, 1024], P(None, 'tp'), may hold values from -0.125 to 0.125
- d_mem: bfloat16 [8192, 1024], P(('grp', 'st'), 'tp'), parts along dimension 0, may hold values from -6 to 6
Outputs:
- d_tokens: bfloat16 [8192, 2048], P(('grp', 'st', 'tp')), parts along dimension 0
- d_store: bfloat16 [128, 64, 2048], P(('grp', 'st', 'tp')), parts along dimension 0
- d_wkey: float32 [4096, 1024], P(('grp', 'st'), 'tp'), parts along dimension 0
There are 2 independent parts, one for each index of `grp`. A program takes and returns all parts, laid end to end along the dimension named above; an argument that names none is the same for every part. Nothing has to cross between parts.
Inputs may be any that keep to these rules, and one draw needn't show every extreme that they name: `pass_ids`: the 8 blocks of one index of st name at most 8 passages (counted with repetition) held by any one index of st o, that is passages o * 16 to o * 16 + 15. Every index of st takes exactly 8 passages from each of 4 indices of st and none from the others, so the bound 8 is reached by every index.
All inputs are finite; a program needn't handle non-finite values.
Results may differ from a plain program's by a relative error of at most 0.02.
Values may be sent and summed in bfloat16 or wider, within the bound.
A program may use at most 128 MiB of HBM per device.

v0:
```python
import functools

import jax
import jax.numpy as jnp
from jax import lax
from jax.experimental import pallas as pl
from jax.experimental.pallas import tpu as pltpu
from jax.sharding import PartitionSpec as P

HD = 256
BLK = 128
PB = 4
BF = jnp.bfloat16
F32 = jnp.float32
MESH = pl.DeviceIdType.MESH
NT = (((1,), (1,)), ((), ()))
TN = (((0,), (0,)), ((), ()))


def dot(a, b, dims=(((1,), (0,)), ((), ()))):
    return lax.dot_general(a, b, dims, preferred_element_type=F32)


def remote(src, dst, send, recv, device):
    return pltpu.make_async_remote_copy(
        src_ref=src,
        dst_ref=dst,
        send_sem=send,
        recv_sem=recv,
        device_id=device,
        device_id_type=MESH,
    )


def tile_of(size, most):
    while size % most:
        most //= 2
    return most


def kernel(
    st_n, tp_n, depth, pass_len,
    slot_ref, req_ref, ask_ref, store_ref, q_hbm, g_hbm, wq_hbm, wg_hbm, wk_hbm, wv_hbm, m_hbm,
    tok_out, store_out, wkey_out,
    rows, wkv, wqg, q_v, g_v, m_v, acc, kv, ask_in, ask_s, out, inc_k, inc_v, ret, prob_v, kvb, reqg, gboth, arr,
    hot, plow, dwp, dwr, tp_part, tp_pair, tp_recv, sp_part, sp_pair, sp_recv,
    lsem, gs, gr, zs, zr, ps, pr, xs, xr,
):
    st = lax.axis_index("st")
    tp = lax.axis_index("tp")
    hi_n = tp_n // 2
    hi, lo = tp // 2, tp % 2
    mate = {"tp": hi * 2 + 1 - lo}
    pass_rows, chunk = rows.shape[1], rows.shape[2]
    model = wqg.shape[0]
    cols = q_v.shape[1]
    heads = cols // HD
    tok_rows = q_v.shape[0]
    blocks = tok_rows // BLK
    blk_keys = PB * pass_len

    def local(i, src, dst):
        copy = pltpu.make_async_copy(src, dst, lsem.at[i])
        copy.start()
        return copy

    own_rows = local(0, store_ref, rows.at[tp])
    loads_kv = [
        local(1, wk_hbm, wkv.at[:, pl.ds(0, cols)]),
        local(2, wv_hbm, wkv.at[:, pl.ds(cols, cols)]),
    ]
    loads_q = [local(3, q_hbm, q_v), local(4, g_hbm, g_v), local(5, m_hbm, m_v)]
    loads_qg = [
        local(6, wq_hbm, wqg.at[:, pl.ds(0, cols)]),
        local(7, wg_hbm, wqg.at[:, pl.ds(cols, cols)]),
    ]

    barrier = pltpu.get_barrier_semaphore()

    def greet_st(d, c):
        pl.semaphore_signal(
            barrier, inc=1, device_id={"st": (st + d) % st_n}, device_id_type=MESH
        )
        return c

    lax.fori_loop(1, st_n, greet_st, 0)
    for d in range(1, tp_n):
        pl.semaphore_signal(
            barrier, inc=1, device_id={"tp": (tp + d) % tp_n}, device_id_type=MESH
        )
    pl.semaphore_wait(barrier, st_n - 1 + tp_n - 1)

    across = []
    for d in range(1, hi_n):
        h = (hi + d) % hi_n
        across.append(
            remote(store_ref, rows.at[tp], gs.at[0, h], gr.at[tp], {"tp": h * 2 + lo})
        )
        across[-1].start()
    beside = remote(store_ref, rows.at[tp], gs.at[1, hi], gr.at[tp], mate)
    beside.start()

    upper = st >= st_n // 2
    mark = jnp.where(upper, st, st_n - 1 - st)

    def far_peer(d):
        i = d - 1
        i = i + jnp.where(i >= mark, 1, 0)
        return jnp.where(upper, i, st_n - 1 - i)

    def z_copy(phase, src, dst, peer):
        return remote(src, dst, zs.at[phase, peer], zr.at[phase, st], {"st": peer})

    def z_wait(phase, src, dst, peer):
        remote(src, dst, zs.at[phase, peer], zr.at[phase, peer], {"st": peer}).wait_recv()

    def ask_send(d, c):
        peer = (st + d) % st_n
        z_copy(0, ask_ref.at[peer], ask_in.at[st], peer).start()
        return c

    lax.fori_loop(1, st_n, ask_send, 0)
    ask_in[st] = ask_ref[st]

    m_tile = tile_of(pass_rows, 256)

    def project(t, first):
        def step(i, c):
            r = pl.ds(pl.multiple_of(i * m_tile, m_tile), m_tile)
            part = dot(rows[t, r], wkv[pl.ds(pl.multiple_of(t * chunk, chunk), chunk), :])
            acc[r] = part if first else acc[r] + part
            return c

        lax.fori_loop(0, pass_rows // m_tile, step, 0)

    def g_wait(t):
        remote(store_ref, rows.at[t], gs.at[1, hi], gr.at[t], mate).wait_recv()

    own_rows.wait()
    for copy in loads_kv:
        copy.wait()
    project(tp, True)
    g_wait(hi * 2 + 1 - lo)
    project(hi * 2 + 1 - lo, False)

    def ask_wait(d, c):
        peer = (st + d) % st_n
        z_wait(0, ask_ref.at[peer], ask_in.at[peer], peer)
        return c

    lax.fori_loop(1, st_n, ask_wait, 0)
    ask_copy = local(8, ask_in, ask_s)
    ask_copy.wait()

    hot_cols = depth * pass_len

    def hot_step(o, c):
        target = ask_in[o][0:1, :hot_cols]
        for i in range(pass_rows // m_tile):
            line = lax.broadcasted_iota(jnp.int32, (m_tile, hot_cols), 0) + i * m_tile
            hot[o, i * m_tile : (i + 1) * m_tile, :] = jnp.where(line == target, 1.0, 0.0).astype(BF)
        return c

    lax.fori_loop(0, st_n, hot_step, 0)
    onward = []
    for d in range(1, hi_n):
        h = (hi + d) % hi_n
        t = h * 2 + lo
        g_wait(t)
        onward.append(remote(rows.at[t], rows.at[t], gs.at[2, h], gr.at[t], mate))
        onward[-1].start()
        project(t, False)
    for d in range(1, hi_n):
        t = ((hi + d) % hi_n) * 2 + 1 - lo
        g_wait(t)
        project(t, False)

    def low_step(i, c):
        kv[i] = acc[pl.ds(pl.multiple_of(i * pass_len, pass_len), pass_len), :].astype(BF)
        return c

    lax.fori_loop(0, pass_rows // pass_len, low_step, 0)

    ks, vs_all = pl.ds(0, cols), pl.ds(cols, cols)

    def half(ref, peer, part):
        return ref.at[peer, :, :, part]

    def key_copy(peer):
        return z_copy(1, half(out, peer, ks), inc_k.at[st], peer)

    def value_copy(peer):
        return z_copy(4, half(out, peer, vs_all), inc_v.at[st], peer)

    def kv_send(d, c):
        peer = far_peer(d)
        for k in range(depth):
            out[peer, k] = kv[ask_s[peer, 1, k]]
        key_copy(peer).start()
        return c

    def value_send(d, c):
        value_copy(far_peer(d)).start()
        return c

    lax.fori_loop(1, st_n, kv_send, 0)
    lax.fori_loop(1, st_n, value_send, 0)
    for k in range(depth):
        picked = kv[ask_s[st, 1, k]]
        inc_k[st, k] = picked[:, :cols]
        inc_v[st, k] = picked[:, cols:]
    for copy in loads_q + loads_qg:
        copy.wait()

    def key_wait(d, c):
        peer = (st + d) % st_n
        z_wait(1, half(out, peer, ks), inc_k.at[peer], peer)
        return c

    lax.fori_loop(1, st_n, key_wait, 0)
    scale = HD ** (-0.5)

    def probs_step(b, c):
        r = pl.ds(pl.multiple_of(b * BLK, BLK), BLK)
        for j in range(PB):
            kvb[j * pass_len : (j + 1) * pass_len, :cols] = inc_k[
                slot_ref[0, b * PB + j], slot_ref[1, b * PB + j]
            ]
        for head in range(heads):
            hs = slice(head * HD, (head + 1) * HD)
            vs = slice(cols + head * HD, cols + (head + 1) * HD)
            gate = g_v[r, hs].astype(F32)
            scores = dot(q_v[r, hs], kvb[:, hs], NT) * scale
            shifted = jnp.exp(scores - jnp.max(scores, axis=-1, keepdims=True))
            prob = shifted / jnp.sum(shifted, axis=-1, keepdims=True)
            prob_v[head, r, :] = prob
            sig = 1.0 / (1.0 + jnp.exp(-gate))
            att_grad = (gate * sig * m_v[r, hs].astype(F32)).astype(BF)
            value_grad = dot(prob.astype(BF), att_grad, TN).astype(BF)
            for j in range(PB):
                reqg[b * PB + j, :, vs] = value_grad[j * pass_len : (j + 1) * pass_len]
        return c

    lax.fori_loop(0, blocks, probs_step, 0)

    def back_copy(phase, part, peer):
        return z_copy(phase, half(ret, peer, part), half(arr, st, part), peer)

    def give_back(phase, part, span):
        def send(d, c):
            peer = far_peer(d)
            for k in range(depth):
                ret[peer, k, :, span] = reqg[req_ref[peer, k]][:, span]
            back_copy(phase, part, peer).start()
            return c

        lax.fori_loop(1, st_n, send, 0)
        for k in range(depth):
            arr[st, k, :, span] = reqg[req_ref[st, k]][:, span]

    give_back(2, vs_all, slice(cols, 2 * cols))

    def value_wait(d, c):
        peer = (st + d) % st_n
        z_wait(4, half(out, peer, vs_all), inc_v.at[peer], peer)
        return c

    lax.fori_loop(1, st_n, value_wait, 0)

    def block_step(b, c):
        r = pl.ds(pl.multiple_of(b * BLK, BLK), BLK)
        for j in range(PB):
            o, k = slot_ref[0, b * PB + j], slot_ref[1, b * PB + j]
            kvb[j * pass_len : (j + 1) * pass_len, :cols] = inc_k[o, k]
            kvb[j * pass_len : (j + 1) * pass_len, cols:] = inc_v[o, k]
        for head in range(heads):
            hs = slice(head * HD, (head + 1) * HD)
            vs = slice(cols + head * HD, cols + (head + 1) * HD)
            q = q_v[r, hs]
            key = kvb[:, hs]
            value = kvb[:, vs]
            gate = g_v[r, hs].astype(F32)
            grad = m_v[r, hs].astype(F32)
            prob = prob_v[head, r, :]
            attended = dot(prob.astype(BF), value)
            sig = 1.0 / (1.0 + jnp.exp(-gate))
            att_grad = (gate * sig * grad).astype(BF)
            gboth[r, vs] = (grad * attended * sig * (1.0 + gate * (1.0 - sig))).astype(BF)
            prob_grad = dot(att_grad, value, NT)
            inner = jnp.sum(prob * prob_grad, axis=-1, keepdims=True)
            score_grad = (scale * prob * (prob_grad - inner)).astype(BF)
            gboth[r, hs] = dot(score_grad, key).astype(BF)
            key_grad = dot(score_grad, q, TN).astype(BF)
            for j in range(PB):
                reqg[b * PB + j, :, hs] = key_grad[j * pass_len : (j + 1) * pass_len]
        return c

    lax.fori_loop(0, blocks, block_step, 0)
    give_back(5, ks, slice(0, cols))

    n_tile = tile_of(model, 512)

    def expand(src, weight, part, pair_rows, t):
        base = pl.multiple_of(t * pair_rows, pair_rows)
        a = src[pl.ds(base, pair_rows), :]

        def step(i, c):
            n = pl.ds(pl.multiple_of(i * n_tile, n_tile), n_tile)
            part[t, :, n] = dot(a, weight[n, :], NT).astype(BF)
            return c

        lax.fori_loop(0, model // n_tile, step, 0)

    def pair_copy(which, part, pair, h):
        return remote(part.at[h * 2 + 1 - lo], pair.at[h], ps.at[which, h], pr.at[which, h], mate)

    def scatter_first(which, src, weight, part, pair, pair_rows):
        for d in range(1, hi_n + 1):
            h = (hi + d) % hi_n
            expand(src, weight, part, pair_rows, h * 2 + 1 - lo)
            pair_copy(which, part, pair, h).start()

    def cross(which, send, recv, h):
        return remote(
            send.at[h * 2 + lo], recv.at[hi], xs.at[which, h], xr.at[which, hi], {"tp": h * 2 + lo}
        )

    def scatter_second(which, src, weight, part, pair, send, recv, pair_rows):
        for d in range(1, hi_n + 1):
            h = (hi + d) % hi_n
            expand(src, weight, part, pair_rows, h * 2 + lo)
            pair_copy(which, part, pair, h).wait_recv()
            if d < hi_n:
                part[h * 2 + lo] = (part[h * 2 + lo].astype(F32) + pair[h].astype(F32)).astype(BF)
                cross(which, part, recv, h).start()

    def scatter_last(which, part, pair, send, recv, result):
        for d in range(1, hi_n):
            h = (hi + d) % hi_n
            remote(
                send.at[h * 2 + lo], recv.at[h], xs.at[which, h], xr.at[which, h], {"tp": h * 2 + lo}
            ).wait_recv()
        total = part[tp].astype(F32) + pair[hi].astype(F32)
        for d in range(1, hi_n):
            total = total + recv[(hi + d) % hi_n].astype(F32)
        result[...] = total.astype(BF)

    tok_pair = tok_rows // tp_n
    sto_pair = pass_rows // tp_n
    scatter_first(0, gboth, wqg, tp_part, tp_pair, tok_pair)
    scatter_second(0, gboth, wqg, tp_part, tp_pair, tp_part, tp_recv, tok_pair)

    def gather_sums(o, span, first):
        def step(i, c):
            r = pl.ds(pl.multiple_of(i * m_tile, m_tile), m_tile)
            part = dot(hot[o, r, :], arr[o, :, :, span].reshape(hot_cols, cols))
            acc[r, span] = part if first else acc[r, span] + part
            return c

        lax.fori_loop(0, pass_rows // m_tile, step, 0)

    for phase, part, span in ((2, vs_all, slice(cols, 2 * cols)), (5, ks, slice(0, cols))):
        gather_sums(st, span, True)

        def grad_wait(d, c):
            peer = (st + d) % st_n
            z_wait(phase, half(ret, peer, part), half(arr, peer, part), peer)
            gather_sums(peer, span, False)
            return c

        lax.fori_loop(1, st_n, grad_wait, 0)
        plow[:, span] = acc[:, span].astype(BF)

    scatter_first(1, plow, wkv, sp_part, sp_pair, sto_pair)

    def wkey_step(t, c):
        dwp[pl.ds(pl.multiple_of(t * chunk, chunk), chunk), :] = dot(
            rows[t], plow[:, :cols], TN
        ).astype(BF)
        return c

    lax.fori_loop(0, tp_n, wkey_step, 0)
    share = model // st_n

    def part_of(s):
        return dwp.at[pl.ds(pl.multiple_of(s * share, share), share), :]

    def wkey_send(d, c):
        peer = far_peer(d)
        z_copy(3, part_of(peer), dwr.at[st], peer).start()
        return c

    lax.fori_loop(1, st_n, wkey_send, 0)
    scatter_second(1, plow, wkv, sp_part, sp_pair, sp_part, sp_recv, sto_pair)
    scatter_last(0, tp_part, tp_pair, tp_part, tp_recv, tok_out)
    wkey_out[...] = part_of(st)[...].astype(F32)

    def wkey_wait(d, c):
        peer = (st + d) % st_n
        z_wait(3, part_of(peer), dwr.at[peer], peer)
        wkey_out[...] += dwr[peer].astype(F32)
        return c

    lax.fori_loop(1, st_n, wkey_wait, 0)
    scatter_last(1, sp_part, sp_pair, sp_part, sp_recv, store_out)

    for copy in across + [beside] + onward:
        copy.wait_send()

    def drain(d, c):
        peer = (st + d) % st_n
        z_copy(0, ask_ref.at[peer], ask_in.at[st], peer).wait_send()
        key_copy(peer).wait_send()
        value_copy(peer).wait_send()
        back_copy(2, vs_all, peer).wait_send()
        back_copy(5, ks, peer).wait_send()
        z_copy(3, part_of(peer), dwr.at[st], peer).wait_send()
        return c

    lax.fori_loop(1, st_n, drain, 0)
    for d in range(1, hi_n + 1):
        h = (hi + d) % hi_n
        pair_copy(0, tp_part, tp_pair, h).wait_send()
        pair_copy(1, sp_part, sp_pair, h).wait_send()
        if d < hi_n:
            cross(0, tp_part, tp_recv, h).wait_send()
            cross(1, sp_part, sp_recv, h).wait_send()


def local(pass_ids, store, queries, gate_pre, w_query, w_gate, w_key, w_value, d_mem):
    st_n = lax.axis_size("st")
    tp_n = lax.axis_size("tp")
    hi_n = tp_n // 2
    tok_rows, cols = queries.shape
    blocks = tok_rows // BLK
    passages, pass_len, chunk = store.shape
    model = w_key.shape[0]
    requests = blocks * PB
    depth = max(2, requests // st_n)
    pass_rows = passages * pass_len
    share = model // st_n

    ids = pass_ids.reshape(-1)
    owners = ids // passages
    within = ids % passages
    order = jnp.arange(requests, dtype=jnp.int32)
    earlier = (owners[None, :] == owners[:, None]) & (order[None, :] < order[:, None])
    rank = jnp.sum(earlier.astype(jnp.int32), axis=1)
    slots = jnp.stack([owners, rank])
    o_i = jnp.arange(st_n, dtype=jnp.int32)[:, None, None]
    k_i = jnp.arange(depth, dtype=jnp.int32)[None, :, None]
    match = (owners[None, None, :] == o_i) & (rank[None, None, :] == k_i)
    asked = jnp.max(jnp.where(match, within[None, None, :], -1), axis=2)
    req_of = jnp.max(jnp.where(match, order[None, None, :], 0), axis=2)
    hot_cols = depth * pass_len
    width = -(-hot_cols // 128) * 128
    lane = jnp.arange(width, dtype=jnp.int32)
    spread = jnp.repeat(asked, pass_len, axis=1)
    spread = jnp.pad(spread, ((0, 0), (0, width - hot_cols)), constant_values=-1)
    target = jnp.where(spread < 0, -1, spread * pass_len + lane[None, :] % pass_len)
    flat = jnp.pad(jnp.maximum(asked, 0), ((0, 0), (0, width - depth)))
    ask = jnp.concatenate(
        [target[:, None], flat[:, None], jnp.zeros((st_n, 6, width), jnp.int32)], axis=1
    )

    vmem = pl.BlockSpec(memory_space=pltpu.VMEM)
    smem = pl.BlockSpec(memory_space=pltpu.SMEM)
    hbm = pl.BlockSpec(memory_space=pl.ANY)
    V = pltpu.VMEM
    DMA = pltpu.SemaphoreType.DMA
    pair = 2 * cols
    tok_pair = tok_rows // tp_n
    sto_pair = pass_rows // tp_n
    d_tokens, d_store, d_wkey = pl.pallas_call(
        functools.partial(kernel, st_n, tp_n, depth, pass_len),
        out_shape=(
            jax.ShapeDtypeStruct((tok_pair, model), BF),
            jax.ShapeDtypeStruct((sto_pair, model), BF),
            jax.ShapeDtypeStruct((share, cols), F32),
        ),
        in_specs=[smem, smem, vmem] + [hbm] * 8,
        out_specs=(vmem, vmem, vmem),
        scratch_shapes=[
            V((tp_n, pass_rows, chunk), BF),
            V((model, pair), BF),
            V((model, pair), BF),
            V((tok_rows, cols), BF),
            V((tok_rows, cols), BF),
            V((tok_rows, cols), BF),
            V((pass_rows, pair), F32),
            V((passages, pass_len, pair), BF),
            V((st_n, 8, width), jnp.int32),
            pltpu.SMEM((st_n, 8, width), jnp.int32),
            V((st_n, depth, pass_len, pair), BF),
            V((st_n, depth, pass_len, cols), BF),
            V((st_n, depth, pass_len, cols), BF),
            V((st_n, depth, pass_len, pair), BF),
            V((cols // HD, tok_rows, PB * pass_len), F32),
            V((PB * pass_len, pair), BF),
            V((requests, pass_len, pair), BF),
            V((tok_rows, pair), BF),
            V((st_n, depth, pass_len, pair), BF),
            V((st_n, pass_rows, hot_cols), BF),
            V((pass_rows, pair), BF),
            V((model, cols), BF),
            V((st_n, share, cols), BF),
            V((tp_n, tok_pair, model), BF),
            V((hi_n, tok_pair, model), BF),
            V((hi_n, tok_pair, model), BF),
            V((tp_n, sto_pair, model), BF),
            V((hi_n, sto_pair, model), BF),
            V((hi_n, sto_pair, model), BF),
            DMA((9,)),
            DMA((3, hi_n)),
            DMA((tp_n,)),
            DMA((6, st_n)),
            DMA((6, st_n)),
            DMA((2, hi_n)),
            DMA((2, hi_n)),
            DMA((2, hi_n)),
            DMA((2, hi_n)),
        ],
        compiler_params=pltpu.CompilerParams(
            collective_id=0, has_side_effects=True, vmem_limit_bytes=67043328
        ),
    )(
        slots, req_of, ask, store.reshape(pass_rows, chunk),
        queries, gate_pre, w_query, w_gate, w_key, w_value, d_mem,
    )
    return d_tokens, d_store.reshape(passages // tp_n, pass_len, model), d_wkey


def solution(mesh):
    return jax.shard_map(
        local,
        mesh=mesh,
        in_specs=(
            P(("grp", "st"), None),
            P("st", None, "tp"),
            P(("grp", "st"), "tp"),
            P(("grp", "st"), "tp"),
            P(None, "tp"),
            P(None, "tp"),
            P(None, "tp"),
            P(None, "tp"),
            P(("grp", "st"), "tp"),
        ),
        out_specs=(
            P(("grp", "st", "tp"), None),
            P(("grp", "st", "tp"), None, None),
            P(("grp", "st"), "tp"),
        ),
        check_vma=False,
    )
```

profile of v0, /device:TPU:8, one launch (start us, length us, event | category | flops | bytes accessed | tf_op | source)
XLA Modules:
  0.0 168.1 jit_solution(11189842651473927074)
XLA Ops:
  0.6 0.0 copy-start.2
  0.7 0.1 pad.7.clone
  0.7 0.6 copy-done.2
  1.3 0.1 copy.17
  1.4 0.1 reshape.279
  1.5 0.1 reshape.278
  1.6 0.2 convert_reduce_fusion
  1.8 0.6 pad_add_fusion.slot_ref
  2.4 0.8 fusion.1
  3.2 0.1 broadcast_in_dim.51
  3.3 0.1 lt.50
  3.4 0.1 broadcast_in_dim.53
  3.4 0.1 mul.19
  3.5 0.7 add_add_fusion.ask_ref
  4.2 159.2 %shard_map.112 = (bf16[256,2048]{1,0:T(8,128)(2,1)}, bf16[256,2048]{1,0:T(8,128)(2,1)}, f32[512,256]{1,0:T(8,128)}) custom-call(s32[2,32]{1,0:T(2,128)} %pad_add_fusion.slot_ref, s32[4,8]{1,0:T(4,128)} %get-tuple-element.10.req_ref, s32[4,8,512]{2,1,0:T(8,128)} %add_add_fusion.ask_ref, bf16[1024,512]{1,0:T(8,128)(2,1)} %bitcast.4, bf16[1024,256]{1,0:T(8,128)(2,1)} %q_hbm.1, ...), custom_call_target="tpu_custom_call" | custom-call | tf_op jit(solution)/shard_map/pallas_call | solution.py:474
  163.5 0.0 copy-start
  163.5 2.4 %copy.23 = bf16[256,2048]{1,0:T(8,128)(2,1)} copy(bf16[256,2048]{1,0:T(8,128)(2,1)} %get-tuple-element.18) | data formatting | bytes 2097152
  165.9 0.0 copy-done
  165.9 0.0 copy-start.1
  165.9 1.0 copy.24
  166.9 0.4 copy-done.1
  167.3 0.8 copy.25
  (11 shorter events, 0.1 us)
Async XLA Ops:
  0.6 0.7 copy-start.2
  163.5 2.4 %copy-start = (bf16[256,2048]{1,0:T(8,128)(2,1)S(1)}, bf16[256,2048]{1,0:T(8,128)(2,1)}, u32[]{:S(2)}) copy-start(bf16[256,2048]{1,0:T(8,128)(2,1)} %get-tuple-element.7) | copy-start | bytes 3145732
  165.9 1.4 copy-start.1
where the time goes:
time: 168 us
  Pallas kernels  159 us (95%)
  local copies, waits for them, and re-layouts  5.83 us (3%)
  other arithmetic  2.32 us (1%)
    pallas_call x1, Pallas kernels, local(): pl.pallas_call(functools.partial(kernel, st_n, tp_n, depth, pass_len), ou...  159 us
    unnamed x10, local copies, waits for them, and re-layouts  5.26 us

commit v1 on v0

--- a/solution.py
+++ b/solution.py
@@ -427,6 +427,598 @@
             cross(1, sp_part, sp_recv, h).wait_send()
 
 
+def gathered_kernel(
+    st_n, tp_n, depth, pass_len,
+    ids_ref, req_ref, ask_ref, store_ref, q_hbm, g_hbm, wq_hbm, wg_hbm, wk_hbm, wv_hbm, m_hbm,
+    tok_out, store_out, wkey_out,
+    rows, wall, wqg, q_v, g_v, m_v, acc, vterm, k_all, v_all, ask_in, ret, prob_v, kvb, reqg, gboth, arr,
+    hot, plow, sums, dwp, dwu, dwd, tp_part, tp_pair, tp_recv,
+    lsem, gs, gr, fs, fr, zs, zr, ps, pr, xs, xr, ws, wr, ss, sr, us, ur,
+):
+    grp = lax.axis_index("grp")
+    st = lax.axis_index("st")
+    tp = lax.axis_index("tp")
+    hi_n = tp_n // 2
+    hi, lo = tp // 2, tp % 2
+    mate_t = hi * 2 + 1 - lo
+    mate = {"tp": mate_t}
+    twin = {"grp": 1 - grp}
+    pass_rows, chunk = rows.shape[1], rows.shape[2]
+    passages = pass_rows // pass_len
+    model = wqg.shape[0]
+    cols = q_v.shape[1]
+    heads = cols // HD
+    tok_rows = q_v.shape[0]
+    blocks = tok_rows // BLK
+    half_pass = passages // 2
+    some = tile_of(half_pass, 2)
+    some_rows = some * pass_len
+    n_some = half_pass // some
+    key_cols, value_cols = slice(0, cols), slice(cols, 2 * cols)
+
+    def local(i, src, dst):
+        copy = pltpu.make_async_copy(src, dst, lsem.at[i])
+        copy.start()
+        return copy
+
+    loads_kv = [
+        local(0, store_ref, rows.at[tp]),
+        local(1, wk_hbm, wall.at[tp, :, pl.ds(0, cols)]),
+        local(2, wv_hbm, wall.at[tp, :, pl.ds(cols, cols)]),
+    ]
+    loads_q = [
+        local(3, q_hbm, q_v),
+        local(4, g_hbm, g_v),
+        local(5, m_hbm, m_v),
+        local(6, wq_hbm, wqg.at[:, pl.ds(0, cols)]),
+        local(7, wg_hbm, wqg.at[:, pl.ds(cols, cols)]),
+    ]
+
+    barrier = pltpu.get_barrier_semaphore()
+
+    def greet_st(d, c):
+        pl.semaphore_signal(
+            barrier, inc=1, device_id={"st": (st + d) % st_n}, device_id_type=MESH
+        )
+        return c
+
+    lax.fori_loop(1, st_n, greet_st, 0)
+    for d in range(1, tp_n):
+        pl.semaphore_signal(
+            barrier, inc=1, device_id={"tp": (tp + d) % tp_n}, device_id_type=MESH
+        )
+    pl.semaphore_signal(barrier, inc=1, device_id=twin, device_id_type=MESH)
+    pl.semaphore_wait(barrier, st_n + tp_n - 1)
+
+    def first_row(i):
+        part = (grp + i // n_some) % 2
+        return pl.multiple_of((part * n_some + i % n_some) * some_rows, some_rows)
+
+    def g_copy(way, i, t, source, peer, slot):
+        r = pl.ds(first_row(i), some_rows)
+        src = store_ref.at[r] if source is None else rows.at[source, r]
+        return remote(src, rows.at[t, r], gs.at[way, slot, i], gr.at[t, i], peer)
+
+    def across(d, i):
+        h = (hi + d) % hi_n
+        return g_copy(0, i, tp, None, {"tp": h * 2 + lo}, h)
+
+    def beside(i):
+        return g_copy(1, i, tp, None, mate, hi)
+
+    def onward(d, i):
+        h = (hi + d) % hi_n
+        return g_copy(2, i, h * 2 + lo, h * 2 + lo, mate, h)
+
+    def g_wait(t, i):
+        g_copy(1, i, t, None, mate, hi).wait_recv()
+
+    def rows_send(i, c):
+        for d in range(1, hi_n):
+            across(d, i).start()
+        beside(i).start()
+        return c
+
+    lax.fori_loop(0, 2 * n_some, rows_send, 0)
+
+    upper = st >= st_n // 2
+    mark = jnp.where(upper, st, st_n - 1 - st)
+
+    def far_peer(d):
+        i = d - 1
+        i = i + jnp.where(i >= mark, 1, 0)
+        return jnp.where(upper, i, st_n - 1 - i)
+
+    def z_copy(phase, src, dst, peer):
+        return remote(src, dst, zs.at[phase, peer], zr.at[phase, st], {"st": peer})
+
+    def z_wait(phase, src, dst, peer):
+        remote(src, dst, zs.at[phase, peer], zr.at[phase, peer], {"st": peer}).wait_recv()
+
+    def ask_send(d, c):
+        peer = (st + d) % st_n
+        z_copy(0, ask_ref.at[peer], ask_in.at[st], peer).start()
+        return c
+
+    lax.fori_loop(1, st_n, ask_send, 0)
+    ask_in[st] = ask_ref[st]
+
+    def project(i):
+        r = pl.ds(first_row(i), some_rows)
+
+        def term(t):
+            w = wall[tp, pl.ds(pl.multiple_of(t * chunk, chunk), chunk), :]
+            return dot(rows[t, r], w)
+
+        for d in range(1, hi_n):
+            g_wait(((hi + d) % hi_n) * 2 + lo, i)
+            onward(d, i).start()
+        g_wait(mate_t, i)
+        total = term(tp) + term(mate_t)
+        for d in range(1, hi_n):
+            total = total + term(((hi + d) % hi_n) * 2 + lo)
+        for d in range(1, hi_n):
+            t = ((hi + d) % hi_n) * 2 + 1 - lo
+            g_wait(t, i)
+            total = total + term(t)
+        low = total.astype(BF)
+        first = st * passages + first_row(i) // pass_len
+        for p in range(some):
+            k_all[first + p] = low[p * pass_len : (p + 1) * pass_len, key_cols]
+            v_all[first + p] = low[p * pass_len : (p + 1) * pass_len, value_cols]
+
+    def part_of_all(kind, o, c, side):
+        ref = k_all if kind == 0 else v_all
+        return ref.at[pl.ds(o * passages + side * half_pass + c * some, some)]
+
+    def chain_copy(kind, o, c, way, peer):
+        part = part_of_all(kind, o, c, grp)
+        return remote(part, part, fs.at[kind, o, c, way], fr.at[kind, o, c, 0], {"st": peer})
+
+    def twin_copy(kind, o, c):
+        part = part_of_all(kind, o, c, grp)
+        return remote(part, part, fs.at[kind, o, c, 2], fr.at[kind, o, c, 1], twin)
+
+    def own_copies(kind, c, act):
+        @pl.when(st + 1 < st_n)
+        def _():
+            act(chain_copy(kind, st, c, 0, st + 1))
+
+        @pl.when(st > 0)
+        def _():
+            act(chain_copy(kind, st, c, 1, st - 1))
+
+    def relay_copies(kind, d, c, act, ready):
+        for way, sign in ((0, -1), (1, 1)):
+            o = st + sign * d
+            onto = st - sign
+
+            @pl.when((o >= 0) & (o < st_n))
+            def _():
+                if ready:
+                    chain_copy(kind, o, c, way, st).wait_recv()
+
+                @pl.when((onto >= 0) & (onto < st_n))
+                def _():
+                    act(chain_copy(kind, o, c, way, onto))
+
+                act(twin_copy(kind, o, c))
+
+    def start(copy):
+        copy.start()
+
+    def own_send(kind, c):
+        own_copies(kind, c, start)
+
+    def relay(kind, d, c):
+        relay_copies(kind, d, c, start, True)
+
+    def twin_wait(kind):
+        def step(i, c):
+            o = (st + 1 + i // n_some) % st_n
+            k = i % n_some
+            part = part_of_all(kind, o, k, 1 - grp)
+            remote(part, part, fs.at[kind, o, k, 2], fr.at[kind, o, k, 1], twin).wait_recv()
+            return c
+
+        lax.fori_loop(0, (st_n - 1) * n_some, step, 0)
+
+    for copy in loads_kv:
+        copy.wait()
+
+    def early_step(i, c):
+        project(i)
+        own_send(0, i)
+
+        @pl.when(i > 0)
+        def _():
+            relay(0, 1, i - 1)
+
+        return c
+
+    lax.fori_loop(0, n_some, early_step, 0)
+    relay(0, 1, n_some - 1)
+
+    def value_send(i, c):
+        own_send(1, i)
+        return c
+
+    lax.fori_loop(0, n_some, value_send, 0)
+
+    def late_step(i, c):
+        project(n_some + i)
+        relay(0, 2, i)
+        return c
+
+    lax.fori_loop(0, n_some, late_step, 0)
+
+    w_half = model // 2
+    w_mine = pl.ds(pl.multiple_of(grp * w_half, w_half), w_half)
+    w_other = pl.ds(pl.multiple_of((1 - grp) * w_half, w_half), w_half)
+
+    def w_across(d):
+        h = (hi + d) % hi_n
+        part = wall.at[tp, w_mine]
+        return remote(part, part, ws.at[0, h], wr.at[0, tp], {"tp": h * 2 + lo})
+
+    def w_twin(d):
+        t = ((hi + d) % hi_n) * 2 + lo
+        part = wall.at[t, w_mine]
+        return remote(part, part, ws.at[1, (hi + d) % hi_n], wr.at[1, t], twin)
+
+    def w_onward(d, k):
+        t = ((hi + d) % hi_n) * 2 + lo
+        part = wall.at[t, w_other if k else w_mine]
+        return remote(part, part, ws.at[2 + k, (hi + d) % hi_n], wr.at[2 + k, t], mate)
+
+    w_beside = remote(wall.at[tp], wall.at[tp], ws.at[4, 0], wr.at[4, tp], mate)
+
+    def w_wait(kind, t, part):
+        remote(wall.at[t, part], wall.at[t, part], ws.at[kind, 0], wr.at[kind, t], mate).wait_recv()
+
+    for d in range(1, hi_n):
+        w_across(d).start()
+    w_beside.start()
+
+    def relay_rest(kind, first, last):
+        def step(i, c):
+            relay(kind, 1 + i // n_some, i % n_some)
+            return c
+
+        lax.fori_loop(first, last, step, 0)
+
+    relays = (st_n - 1) * n_some
+    relay_rest(0, 2 * n_some, relays)
+    for copy in loads_q:
+        copy.wait()
+    twin_wait(0)
+    scale = HD ** (-0.5)
+
+    def fill(ref, span, b):
+        for j in range(PB):
+            kvb[j * pass_len : (j + 1) * pass_len, span] = ref[ids_ref[b * PB + j]]
+
+    def probs_step(b, c):
+        r = pl.ds(pl.multiple_of(b * BLK, BLK), BLK)
+        fill(k_all, key_cols, b)
+        for head in range(heads):
+            hs = slice(head * HD, (head + 1) * HD)
+            vs = slice(cols + head * HD, cols + (head + 1) * HD)
+            gate = g_v[r, hs].astype(F32)
+            scores = dot(q_v[r, hs], kvb[:, hs], NT) * scale
+            shifted = jnp.exp(scores - jnp.max(scores, axis=-1, keepdims=True))
+            prob = shifted / jnp.sum(shifted, axis=-1, keepdims=True)
+            prob_v[head, r, :] = prob
+            sig = 1.0 / (1.0 + jnp.exp(-gate))
+            att_grad = (gate * sig * m_v[r, hs].astype(F32)).astype(BF)
+            value_grad = dot(prob.astype(BF), att_grad, TN).astype(BF)
+            for j in range(PB):
+                reqg[b * PB + j, :, vs] = value_grad[j * pass_len : (j + 1) * pass_len]
+
+        @pl.when(b < relays)
+        def _():
+            relay(1, 1 + b // n_some, b % n_some)
+
+        return c
+
+    lax.fori_loop(0, blocks, probs_step, 0)
+
+    def half(ref, peer, part):
+        return ref.at[peer, :, :, part]
+
+    def back_copy(phase, part, peer):
+        return z_copy(phase, half(ret, peer, part), half(arr, st, part), peer)
+
+    def give_back(phase, part, span):
+        def send(d, c):
+            peer = far_peer(d)
+            for k in range(depth):
+                ret[peer, k, :, span] = reqg[req_ref[peer, k]][:, span]
+            back_copy(phase, part, peer).start()
+            return c
+
+        lax.fori_loop(1, st_n, send, 0)
+        for k in range(depth):
+            arr[st, k, :, span] = reqg[req_ref[st, k]][:, span]
+
+    ks, vs_all = pl.ds(0, cols), pl.ds(cols, cols)
+    give_back(1, vs_all, value_cols)
+    relay_rest(1, min(blocks, relays), relays)
+    twin_wait(1)
+
+    def block_step(b, c):
+        r = pl.ds(pl.multiple_of(b * BLK, BLK), BLK)
+        fill(k_all, key_cols, b)
+        fill(v_all, value_cols, b)
+        for head in range(heads):
+            hs = slice(head * HD, (head + 1) * HD)
+            vs = slice(cols + head * HD, cols + (head + 1) * HD)
+            q = q_v[r, hs]
+            key = kvb[:, hs]
+            value = kvb[:, vs]
+            gate = g_v[r, hs].astype(F32)
+            grad = m_v[r, hs].astype(F32)
+            prob = prob_v[head, r, :]
+            attended = dot(prob.astype(BF), value)
+            sig = 1.0 / (1.0 + jnp.exp(-gate))
+            att_grad = (gate * sig * grad).astype(BF)
+            gboth[r, vs] = (grad * attended * sig * (1.0 + gate * (1.0 - sig))).astype(BF)
+            prob_grad = dot(att_grad, value, NT)
+            inner = jnp.sum(prob * prob_grad, axis=-1, keepdims=True)
+            score_grad = (scale * prob * (prob_grad - inner)).astype(BF)
+            gboth[r, hs] = dot(score_grad, key).astype(BF)
+            key_grad = dot(score_grad, q, TN).astype(BF)
+            for j in range(PB):
+                reqg[b * PB + j, :, hs] = key_grad[j * pass_len : (j + 1) * pass_len]
+        return c
+
+    lax.fori_loop(0, blocks, block_step, 0)
+    give_back(2, ks, key_cols)
+
+    for d in range(1, hi_n):
+        w_wait(0, ((hi + d) % hi_n) * 2 + lo, w_mine)
+        w_twin(d).start()
+        w_onward(d, 0).start()
+
+    n_tile = tile_of(model, 512)
+
+    def expand(t):
+        a = gboth[pl.ds(pl.multiple_of(t * tok_pair, tok_pair), tok_pair), :]
+
+        def step(i, c):
+            n = pl.ds(pl.multiple_of(i * n_tile, n_tile), n_tile)
+            tp_part[t, :, n] = dot(a, wqg[n, :], NT).astype(BF)
+            return c
+
+        lax.fori_loop(0, model // n_tile, step, 0)
+
+    def pair_copy(h):
+        return remote(tp_part.at[h * 2 + 1 - lo], tp_pair.at[h], ps.at[h], pr.at[h], mate)
+
+    def cross(h):
+        return remote(
+            tp_part.at[h * 2 + lo], tp_recv.at[hi], xs.at[h], xr.at[hi], {"tp": h * 2 + lo}
+        )
+
+    tok_pair = tok_rows // tp_n
+    for d in range(1, hi_n + 1):
+        h = (hi + d) % hi_n
+        expand(h * 2 + 1 - lo)
+        pair_copy(h).start()
+    for d in range(1, hi_n + 1):
+        h = (hi + d) % hi_n
+        expand(h * 2 + lo)
+        pair_copy(h).wait_recv()
+        if d < hi_n:
+            tp_part[h * 2 + lo] = (tp_part[h * 2 + lo].astype(F32) + tp_pair[h].astype(F32)).astype(BF)
+            cross(h).start()
+
+    def ask_wait(d, c):
+        peer = (st + d) % st_n
+        z_wait(0, ask_ref.at[peer], ask_in.at[peer], peer)
+        return c
+
+    lax.fori_loop(1, st_n, ask_wait, 0)
+    hot_cols = depth * pass_len
+    m_tile = tile_of(pass_rows, 256)
+
+    def hot_step(o, c):
+        target = ask_in[o][0:1, :hot_cols]
+        for i in range(pass_rows // m_tile):
+            line = lax.broadcasted_iota(jnp.int32, (m_tile, hot_cols), 0) + i * m_tile
+            hot[o, i * m_tile : (i + 1) * m_tile, :] = jnp.where(line == target, 1.0, 0.0).astype(BF)
+        return c
+
+    lax.fori_loop(0, st_n, hot_step, 0)
+
+    def gather_sums(o, span, first):
+        def step(i, c):
+            r = pl.ds(pl.multiple_of(i * m_tile, m_tile), m_tile)
+            part = dot(hot[o, r, :], arr[o, :, :, span].reshape(hot_cols, cols))
+            acc[r, :] = part if first else acc[r, :] + part
+            return c
+
+        lax.fori_loop(0, pass_rows // m_tile, step, 0)
+
+    sto_pair = pass_rows // tp_n
+
+    def sums_copy(kind, part, d):
+        t = (tp + d) % tp_n
+        src = plow.at[pl.ds(pl.multiple_of(t * sto_pair, sto_pair), sto_pair), part]
+        return remote(src, sums.at[tp, :, part], ss.at[kind, t], sr.at[kind, tp], {"tp": t})
+
+    def sums_wait(kind, part, t):
+        dst = sums.at[t, :, part]
+        remote(dst, dst, ss.at[kind, t], sr.at[kind, t], mate).wait_recv()
+
+    def collect(phase, kind, part, span):
+        gather_sums(st, span, True)
+
+        def grad_wait(d, c):
+            peer = (st + d) % st_n
+            z_wait(phase, half(ret, peer, part), half(arr, peer, part), peer)
+            gather_sums(peer, span, False)
+            return c
+
+        lax.fori_loop(1, st_n, grad_wait, 0)
+        plow[:, span] = acc[...].astype(BF)
+        for d in range(1, tp_n):
+            sums_copy(kind, part, d).start()
+        sums[tp, :, span] = plow[pl.ds(pl.multiple_of(tp * sto_pair, sto_pair), sto_pair), span]
+
+    collect(1, 1, vs_all, value_cols)
+
+    for d in range(1, hi_n):
+        w_wait(1, ((hi + d) % hi_n) * 2 + lo, w_other)
+        w_onward(d, 1).start()
+    w_wait(4, mate_t, pl.ds(0, model))
+    for d in range(1, hi_n):
+        t = ((hi + d) % hi_n) * 2 + 1 - lo
+        w_wait(2, t, w_mine)
+        w_wait(3, t, w_other)
+
+    for d in range(1, hi_n):
+        h = (hi + d) % hi_n
+        remote(
+            tp_part.at[h * 2 + lo], tp_recv.at[h], xs.at[h], xr.at[h], {"tp": h * 2 + lo}
+        ).wait_recv()
+    total = tp_part[tp].astype(F32) + tp_pair[hi].astype(F32)
+    for d in range(1, hi_n):
+        total = total + tp_recv[(hi + d) % hi_n].astype(F32)
+    tok_out[...] = total.astype(BF)
+
+    def store_terms(span, done):
+        def step(i, c):
+            n = pl.ds(pl.multiple_of(i * n_tile, n_tile), n_tile)
+            part = dot(sums[0, :, span], wall[0, n, span], NT)
+            for t in range(1, tp_n):
+                part = part + dot(sums[t, :, span], wall[t, n, span], NT)
+            done(n, part)
+            return c
+
+        lax.fori_loop(0, model // n_tile, step, 0)
+
+    def keep_values(n, part):
+        vterm[:, n] = part
+
+    def keep_store(n, part):
+        store_out[:, n] = (vterm[:, n] + part).astype(BF)
+
+    for d in range(1, tp_n):
+        sums_wait(1, vs_all, (tp + d) % tp_n)
+    store_terms(value_cols, keep_values)
+
+    collect(2, 0, ks, key_cols)
+
+    def wkey_step(t, c):
+        dwp[pl.ds(pl.multiple_of(t * chunk, chunk), chunk), :] = dot(
+            rows[t], plow[:, key_cols], TN
+        ).astype(BF)
+        return c
+
+    lax.fori_loop(0, tp_n, wkey_step, 0)
+    share = model // st_n
+    bits = 2
+    bit = share // bits
+
+    def dw_copy(way, s, b, whole):
+        ref = dwu if way == 0 else dwd
+        line = pl.ds(b * bit, bit)
+        src = dwp.at[pl.ds(pl.multiple_of(s * share + b * bit, bit), bit), :] if whole else ref.at[s, line]
+        peer = st + 1 if way == 0 else st - 1
+        return remote(src, ref.at[s, line], us.at[way, s, b], ur.at[way, s, b], {"st": peer})
+
+    def dw_wait(way, s, b):
+        dw_copy(way, s, b, False).wait_recv()
+
+    def dw_own(s, b):
+        return dwp[pl.ds(pl.multiple_of(s * share + b * bit, bit), bit), :].astype(F32)
+
+    def dw_each(edge, act):
+        for j in range(st_n - 1):
+            for b in range(bits):
+                for way, s in ((0, st_n - 1 - j), (1, j)):
+                    at_edge = st == (0 if way == 0 else st_n - 1)
+                    goes = (s > st) if way == 0 else (s < st)
+
+                    @pl.when(goes & (at_edge if edge else jnp.logical_not(at_edge)))
+                    def _():
+                        act(way, s, b)
+
+    def dw_first(way, s, b):
+        dw_copy(way, s, b, True).start()
+
+    def dw_relay(way, s, b):
+        dw_wait(way, s, b)
+        ref = dwu if way == 0 else dwd
+        line = slice(b * bit, (b + 1) * bit)
+        ref[s, line, :] = (ref[s, line, :].astype(F32) + dw_own(s, b)).astype(BF)
+        dw_copy(way, s, b, False).start()
+
+    dw_each(True, dw_first)
+
+    for d in range(1, tp_n):
+        sums_wait(0, ks, (tp + d) % tp_n)
+    store_terms(key_cols, keep_store)
+
+    dw_each(False, dw_relay)
+    for b in range(bits):
+        line = slice(b * bit, (b + 1) * bit)
+        wkey_out[line, :] = dw_own(st, b)
+        for way, there in ((0, st > 0), (1, st + 1 < st_n)):
+            @pl.when(there)
+            def _():
+                dw_wait(way, st, b)
+                ref = dwu if way == 0 else dwd
+                wkey_out[line, :] += ref[st, line, :].astype(F32)
+
+    def wait_send(copy):
+        copy.wait_send()
+
+    def rows_drain(i, c):
+        for d in range(1, hi_n):
+            across(d, i).wait_send()
+            onward(d, i).wait_send()
+        beside(i).wait_send()
+        return c
+
+    lax.fori_loop(0, 2 * n_some, rows_drain, 0)
+
+    def all_drain(i, c):
+        for kind in (0, 1):
+            own_copies(kind, i, wait_send)
+            for d in range(1, st_n):
+                relay_copies(kind, d, i, wait_send, False)
+        return c
+
+    lax.fori_loop(0, n_some, all_drain, 0)
+    for d in range(1, hi_n):
+        w_across(d).wait_send()
+        w_twin(d).wait_send()
+        w_onward(d, 0).wait_send()
+        w_onward(d, 1).wait_send()
+    w_beside.wait_send()
+
+    def drain(d, c):
+        peer = (st + d) % st_n
+        z_copy(0, ask_ref.at[peer], ask_in.at[st], peer).wait_send()
+        back_copy(1, vs_all, peer).wait_send()
+        back_copy(2, ks, peer).wait_send()
+        return c
+
+    lax.fori_loop(1, st_n, drain, 0)
+    for d in range(1, tp_n):
+        sums_copy(0, ks, d).wait_send()
+        sums_copy(1, vs_all, d).wait_send()
+    for d in range(1, hi_n + 1):
+        h = (hi + d) % hi_n
+        pair_copy(h).wait_send()
+        if d < hi_n:
+            cross(h).wait_send()
+    dw_each(True, lambda way, s, b: dw_copy(way, s, b, True).wait_send())
+    dw_each(False, lambda way, s, b: dw_copy(way, s, b, False).wait_send())
+
+
 def local(pass_ids, store, queries, gate_pre, w_query, w_gate, w_key, w_value, d_mem):
     st_n = lax.axis_size("st")
     tp_n = lax.axis_size("tp")
@@ -471,6 +1063,72 @@
     pair = 2 * cols
     tok_pair = tok_rows // tp_n
     sto_pair = pass_rows // tp_n
+    gathered_bytes = 2 * 2 * st_n * pass_rows * cols
+    if lax.axis_size("grp") == 2 and hi_n == 2 and passages % 2 == 0 and gathered_bytes <= 8 << 20:
+        half_pass = passages // 2
+        n_some = half_pass // tile_of(half_pass, 2)
+        d_tokens, d_store, d_wkey = pl.pallas_call(
+            functools.partial(gathered_kernel, st_n, tp_n, depth, pass_len),
+            out_shape=(
+                jax.ShapeDtypeStruct((tok_pair, model), BF),
+                jax.ShapeDtypeStruct((sto_pair, model), BF),
+                jax.ShapeDtypeStruct((share, cols), F32),
+            ),
+            in_specs=[smem, smem, vmem] + [hbm] * 8,
+            out_specs=(vmem, vmem, vmem),
+            scratch_shapes=[
+                V((tp_n, pass_rows, chunk), BF),
+                V((tp_n, model, pair), BF),
+                V((model, pair), BF),
+                V((tok_rows, cols), BF),
+                V((tok_rows, cols), BF),
+                V((tok_rows, cols), BF),
+                V((pass_rows, cols), F32),
+                V((sto_pair, model), F32),
+                V((st_n * passages, pass_len, cols), BF),
+                V((st_n * passages, pass_len, cols), BF),
+                V((st_n, 8, width), jnp.int32),
+                V((st_n, depth, pass_len, pair), BF),
+                V((cols // HD, tok_rows, PB * pass_len), F32),
+                V((PB * pass_len, pair), BF),
+                V((requests, pass_len, pair), BF),
+                V((tok_rows, pair), BF),
+                V((st_n, depth, pass_len, pair), BF),
+                V((st_n, pass_rows, hot_cols), BF),
+                V((pass_rows, pair), BF),
+                V((tp_n, sto_pair, pair), BF),
+                V((model, cols), BF),
+                V((st_n, share, cols), BF),
+                V((st_n, share, cols), BF),
+                V((tp_n, tok_pair, model), BF),
+                V((hi_n, tok_pair, model), BF),
+                V((hi_n, tok_pair, model), BF),
+                DMA((8,)),
+                DMA((3, hi_n, 2 * n_some)),
+                DMA((tp_n, 2 * n_some)),
+                DMA((2, st_n, n_some, 3)),
+                DMA((2, st_n, n_some, 2)),
+                DMA((3, st_n)),
+                DMA((3, st_n)),
+                DMA((hi_n,)),
+                DMA((hi_n,)),
+                DMA((hi_n,)),
+                DMA((hi_n,)),
+                DMA((5, hi_n)),
+                DMA((5, tp_n)),
+                DMA((2, tp_n)),
+                DMA((2, tp_n)),
+                DMA((2, st_n, 2)),
+                DMA((2, st_n, 2)),
+            ],
+            compiler_params=pltpu.CompilerParams(
+                collective_id=0, has_side_effects=True, vmem_limit_bytes=67043328
+            ),
+        )(
+            ids, req_of, ask, store.reshape(pass_rows, chunk),
+            queries, gate_pre, w_query, w_gate, w_key, w_value, d_mem,
+        )
+        return d_tokens, d_store.reshape(passages // tp_n, pass_len, model), d_wkey
     d_tokens, d_store, d_wkey = pl.pallas_call(
         functools.partial(kernel, st_n, tp_n, depth, pass_len),
         out_shape=(

time: 168 us -> 151 us (0.90)
  the two profiles are of different devices: /device:TPU:8 before, /device:TPU:1 now
where the time goes in v1:
time: 151 us; the launch traced here: 150 us
  Pallas kernels  141 us (93%)
  local copies, waits for them, and re-layouts  6.25 us (4%)
  other arithmetic  1.74 us (1%)
    pallas_call x1, Pallas kernels, local(): pl.pallas_call(functools.partial(gathered_kernel, st_n, tp_n, depth, pass...  141 us
    unnamed x12, local copies, waits for them, and re-layouts  5.76 us

profile of v1, /device:TPU:1, one launch (start us, length us, event | category | flops | bytes accessed | tf_op | source)
XLA Modules:
  0.0 150.2 jit_solution(8836612708473899086)
XLA Ops:
  0.6 0.0 copy-start.3
  0.7 0.1 pad.7.clone
  0.7 0.6 copy-done.3
  1.3 0.1 copy.15
  1.4 0.1 reshape.230.ids_ref
  1.5 0.0 copy-start.2
  1.5 0.5 copy-done.2
  2.0 0.2 convert_reduce_fusion
  2.2 0.8 fusion.1
  3.0 0.1 broadcast_in_dim.51
  3.1 0.1 lt.50
  3.2 0.1 broadcast_in_dim.53
  3.3 0.1 mul.19
  3.4 0.7 add_add_fusion.ask_ref
  4.1 141.5 %shard_map.112 = (bf16[256,2048]{1,0:T(8,128)(2,1)}, bf16[256,2048]{1,0:T(8,128)(2,1)}, f32[512,256]{1,0:T(8,128)}) custom-call(s32[32]{0:T(128)} %copy-done.2, s32[4,8]{1,0:T(4,128)} %get-tuple-element.10.req_ref, s32[4,8,512]{2,1,0:T(8,128)} %add_add_fusion.ask_ref, bf16[1024,512]{1,0:T(8,128)(2,1)} %bitcast.2, bf16[1024,256]{1,0:T(8,128)(2,1)} %q_hbm.1, ...), custom_call_target="tpu_custom_call" | custom-call | tf_op jit(solution)/shard_map/pallas_call | solution.py:1070
  145.6 0.0 copy-start
  145.6 2.4 %copy.20 = bf16[256,2048]{1,0:T(8,128)(2,1)} copy(bf16[256,2048]{1,0:T(8,128)(2,1)} %get-tuple-element.18) | data formatting | bytes 2097152
  148.0 0.0 copy-done
  148.0 0.0 copy-start.1
  148.0 1.0 copy.21
  148.9 0.4 copy-done.1
  149.4 0.8 copy.22
  (10 shorter events, 0.1 us)
Async XLA Ops:
  0.6 0.7 copy-start.3
  1.5 0.5 copy-start.2
  145.6 2.4 %copy-start = (bf16[256,2048]{1,0:T(8,128)(2,1)S(1)}, bf16[256,2048]{1,0:T(8,128)(2,1)}, u32[]{:S(2)}) copy-start(bf16[256,2048]{1,0:T(8,128)(2,1)} %get-tuple-element.7) | copy-start | bytes 3145732
  148.0 1.4 copy-start.1

commit v2 on v1

--- a/solution.py
+++ b/solution.py
@@ -432,7 +432,7 @@
     ids_ref, req_ref, ask_ref, store_ref, q_hbm, g_hbm, wq_hbm, wg_hbm, wk_hbm, wv_hbm, m_hbm,
     tok_out, store_out, wkey_out,
     rows, wall, wqg, q_v, g_v, m_v, acc, vterm, k_all, v_all, ask_in, ret, prob_v, kvb, reqg, gboth, arr,
-    hot, plow, sums, dwp, dwu, dwd, tp_part, tp_pair, tp_recv,
+    hot, plow, sums, dwp, dwc, dwf, tp_part, tp_pair, tp_recv,
     lsem, gs, gr, fs, fr, zs, zr, ps, pr, xs, xr, ws, wr, ss, sr, us, ur,
 ):
     grp = lax.axis_index("grp")
@@ -579,14 +579,20 @@
         part = part_of_all(kind, o, c, grp)
         return remote(part, part, fs.at[kind, o, c, 2], fr.at[kind, o, c, 1], twin)
 
-    def own_copies(kind, c, act):
-        @pl.when(st + 1 < st_n)
-        def _():
-            act(chain_copy(kind, st, c, 0, st + 1))
-
-        @pl.when(st > 0)
-        def _():
-            act(chain_copy(kind, st, c, 1, st - 1))
+    lower = st < st_n // 2
+
+    def own_copies(kind, c, act, inward=True, outward=True):
+        ways = ((0, st + 1, lower), (1, st - 1, jnp.logical_not(lower)))
+        for way, onto, toward in ways:
+            there = (onto >= 0) & (onto < st_n)
+            if not outward:
+                there = there & toward
+            if not inward:
+                there = there & jnp.logical_not(toward)
+
+            @pl.when(there)
+            def _():
+                act(chain_copy(kind, st, c, way, onto))
 
     def relay_copies(kind, d, c, act, ready):
         for way, sign in ((0, -1), (1, 1)):
@@ -607,8 +613,8 @@
     def start(copy):
         copy.start()
 
-    def own_send(kind, c):
-        own_copies(kind, c, start)
+    def own_send(kind, c, **which):
+        own_copies(kind, c, start, **which)
 
     def relay(kind, d, c):
         relay_copies(kind, d, c, start, True)
@@ -639,11 +645,15 @@
     lax.fori_loop(0, n_some, early_step, 0)
     relay(0, 1, n_some - 1)
 
-    def value_send(i, c):
-        own_send(1, i)
-        return c
-
-    lax.fori_loop(0, n_some, value_send, 0)
+    def inward_send(i, c):
+        own_send(1, i, outward=False)
+        return c
+
+    def outward_send(i, c):
+        own_send(1, i, inward=False)
+        return c
+
+    lax.fori_loop(0, n_some, inward_send, 0)
 
     def late_step(i, c):
         project(n_some + i)
@@ -651,6 +661,7 @@
         return c
 
     lax.fori_loop(0, n_some, late_step, 0)
+    lax.fori_loop(0, n_some, outward_send, 0)
 
     w_half = model // 2
     w_mine = pl.ds(pl.multiple_of(grp * w_half, w_half), w_half)
@@ -688,6 +699,8 @@
         lax.fori_loop(first, last, step, 0)
 
     relays = (st_n - 1) * n_some
+    ahead = jnp.where((st > 0) & (st < st_n - 1), n_some, 0)
+    relay_rest(1, 0, ahead)
     relay_rest(0, 2 * n_some, relays)
     for copy in loads_q:
         copy.wait()
@@ -715,9 +728,11 @@
             for j in range(PB):
                 reqg[b * PB + j, :, vs] = value_grad[j * pass_len : (j + 1) * pass_len]
 
-        @pl.when(b < relays)
+        i = ahead + b
+
+        @pl.when(i < relays)
         def _():
-            relay(1, 1 + b // n_some, b % n_some)
+            relay(1, 1 + i // n_some, i % n_some)
 
         return c
 
@@ -743,7 +758,7 @@
 
     ks, vs_all = pl.ds(0, cols), pl.ds(cols, cols)
     give_back(1, vs_all, value_cols)
-    relay_rest(1, min(blocks, relays), relays)
+    relay_rest(1, jnp.minimum(ahead + blocks, relays), relays)
     twin_wait(1)
 
     def block_step(b, c):
@@ -868,6 +883,71 @@
 
     collect(1, 1, vs_all, value_cols)
 
+    collect(2, 0, ks, key_cols)
+
+    share = model // st_n
+    bits = 2
+    bit = share // bits
+    beyond = jnp.where(lower, st_n - 1, 0)
+    middle = jnp.where(lower, st_n // 2, st_n // 2 - 1)
+    beside_st = st + 1 - 2 * (st % 2)
+    outer = (st == 0) | (st == st_n - 1)
+    inner = jnp.logical_not(outer)
+
+    def dw_line(s, b):
+        return pl.ds(pl.multiple_of(s * share + b * bit, bit), bit)
+
+    def dw_copy(kind, b):
+        line = pl.ds(b * bit, bit)
+        if kind < 2:
+            src, dst = dwp.at[dw_line(middle if kind else beyond, b)], dwc.at[kind, line]
+            peer = beside_st
+        elif kind == 2:
+            src, dst, peer = dwp.at[dw_line(beside_st, b)], dwf.at[0, line], beside_st
+        else:
+            src, dst = dwc.at[kind - 3, line], dwf.at[1, line]
+            peer = middle if kind == 4 else beyond
+        return remote(src, dst, us.at[kind, b], ur.at[kind, b], {"st": peer})
+
+    def dw_send(kind):
+        for b in range(bits):
+            dw_copy(kind, b).start()
+
+    def dw_relay(q):
+        for b in range(bits):
+            line = slice(b * bit, (b + 1) * bit)
+            dw_copy(q, b).wait_recv()
+            own = dwp[dw_line(middle if q else beyond, b), :].astype(F32)
+            dwc[q, line, :] = (dwc[q, line, :].astype(F32) + own).astype(BF)
+            dw_copy(3 + q, b).start()
+
+    def wkey_step(s):
+        dwp[pl.ds(pl.multiple_of(s * chunk, chunk), chunk), :] = dot(
+            rows[s], plow[:, key_cols], TN
+        ).astype(BF)
+
+    def wkey_turn(j, c):
+        far = jnp.where(j == 0, beyond, middle)
+        near = jnp.where(j == 2, beside_st, st)
+        near_first = jnp.where(j == 0, beside_st, st)
+        far_after = jnp.where(j == 1, beyond, middle)
+        s = jnp.where(
+            outer, jnp.where(j < 2, far, near), jnp.where((j == 0) | (j == 3), near_first, far_after)
+        )
+        wkey_step(s)
+        for kind in range(3):
+            @pl.when(outer & (j == kind))
+            def _():
+                dw_send(kind)
+
+        @pl.when(inner & (j == 0))
+        def _():
+            dw_send(2)
+
+        return c
+
+    lax.fori_loop(0, st_n, wkey_turn, 0)
+
     for d in range(1, hi_n):
         w_wait(1, ((hi + d) % hi_n) * 2 + lo, w_other)
         w_onward(d, 1).start()
@@ -876,6 +956,35 @@
         t = ((hi + d) % hi_n) * 2 + 1 - lo
         w_wait(2, t, w_mine)
         w_wait(3, t, w_other)
+
+    def store_terms(span, done):
+        def step(i, c):
+            n = pl.ds(pl.multiple_of(i * n_tile, n_tile), n_tile)
+            part = dot(sums[0, :, span], wall[0, n, span], NT)
+            for t in range(1, tp_n):
+                part = part + dot(sums[t, :, span], wall[t, n, span], NT)
+            done(n, part)
+            return c
+
+        lax.fori_loop(0, model // n_tile, step, 0)
+
+    def keep_values(n, part):
+        vterm[:, n] = part
+
+    def keep_store(n, part):
+        store_out[:, n] = (vterm[:, n] + part).astype(BF)
+
+    for d in range(1, tp_n):
+        sums_wait(1, vs_all, (tp + d) % tp_n)
+    store_terms(value_cols, keep_values)
+
+    @pl.when(inner)
+    def _():
+        dw_relay(0)
+
+    for d in range(1, tp_n):
+        sums_wait(0, ks, (tp + d) % tp_n)
+    store_terms(key_cols, keep_store)
 
     for d in range(1, hi_n):
         h = (hi + d) % hi_n
@@ -887,90 +996,22 @@
         total = total + tp_recv[(hi + d) % hi_n].astype(F32)
     tok_out[...] = total.astype(BF)
 
-    def store_terms(span, done):
-        def step(i, c):
-            n = pl.ds(pl.multiple_of(i * n_tile, n_tile), n_tile)
-            part = dot(sums[0, :, span], wall[0, n, span], NT)
-            for t in range(1, tp_n):
-                part = part + dot(sums[t, :, span], wall[t, n, span], NT)
-            done(n, part)
-            return c
-
-        lax.fori_loop(0, model // n_tile, step, 0)
-
-    def keep_values(n, part):
-        vterm[:, n] = part
-
-    def keep_store(n, part):
-        store_out[:, n] = (vterm[:, n] + part).astype(BF)
-
-    for d in range(1, tp_n):
-        sums_wait(1, vs_all, (tp + d) % tp_n)
-    store_terms(value_cols, keep_values)
-
-    collect(2, 0, ks, key_cols)
-
-    def wkey_step(t, c):
-        dwp[pl.ds(pl.multiple_of(t * chunk, chunk), chunk), :] = dot(
-            rows[t], plow[:, key_cols], TN
-        ).astype(BF)
-        return c
-
-    lax.fori_loop(0, tp_n, wkey_step, 0)
-    share = model // st_n
-    bits = 2
-    bit = share // bits
-
-    def dw_copy(way, s, b, whole):
-        ref = dwu if way == 0 else dwd
-        line = pl.ds(b * bit, bit)
-        src = dwp.at[pl.ds(pl.multiple_of(s * share + b * bit, bit), bit), :] if whole else ref.at[s, line]
-        peer = st + 1 if way == 0 else st - 1
-        return remote(src, ref.at[s, line], us.at[way, s, b], ur.at[way, s, b], {"st": peer})
-
-    def dw_wait(way, s, b):
-        dw_copy(way, s, b, False).wait_recv()
-
-    def dw_own(s, b):
-        return dwp[pl.ds(pl.multiple_of(s * share + b * bit, bit), bit), :].astype(F32)
-
-    def dw_each(edge, act):
-        for j in range(st_n - 1):
-            for b in range(bits):
-                for way, s in ((0, st_n - 1 - j), (1, j)):
-                    at_edge = st == (0 if way == 0 else st_n - 1)
-                    goes = (s > st) if way == 0 else (s < st)
-
-                    @pl.when(goes & (at_edge if edge else jnp.logical_not(at_edge)))
-                    def _():
-                        act(way, s, b)
-
-    def dw_first(way, s, b):
-        dw_copy(way, s, b, True).start()
-
-    def dw_relay(way, s, b):
-        dw_wait(way, s, b)
-        ref = dwu if way == 0 else dwd
-        line = slice(b * bit, (b + 1) * bit)
-        ref[s, line, :] = (ref[s, line, :].astype(F32) + dw_own(s, b)).astype(BF)
-        dw_copy(way, s, b, False).start()
-
-    dw_each(True, dw_first)
-
-    for d in range(1, tp_n):
-        sums_wait(0, ks, (tp + d) % tp_n)
-    store_terms(key_cols, keep_store)
-
-    dw_each(False, dw_relay)
+    @pl.when(inner)
+    def _():
+        dw_relay(1)
+
     for b in range(bits):
         line = slice(b * bit, (b + 1) * bit)
-        wkey_out[line, :] = dw_own(st, b)
-        for way, there in ((0, st > 0), (1, st + 1 < st_n)):
-            @pl.when(there)
+        dw_copy(2, b).wait_recv()
+        wkey_out[line, :] = dwp[dw_line(st, b), :].astype(F32) + dwf[0, line, :].astype(F32)
+    for b in range(bits):
+        line = slice(b * bit, (b + 1) * bit)
+        for kind, edge in ((3, outer), (4, inner)):
+            @pl.when(edge)
             def _():
-                dw_wait(way, st, b)
-                ref = dwu if way == 0 else dwd
-                wkey_out[line, :] += ref[st, line, :].astype(F32)
+                dw_copy(kind, b).wait_recv()
+
+        wkey_out[line, :] += dwf[1, line, :].astype(F32)
 
     def wait_send(copy):
         copy.wait_send()
@@ -1015,8 +1056,16 @@
         pair_copy(h).wait_send()
         if d < hi_n:
             cross(h).wait_send()
-    dw_each(True, lambda way, s, b: dw_copy(way, s, b, True).wait_send())
-    dw_each(False, lambda way, s, b: dw_copy(way, s, b, False).wait_send())
+    for b in range(bits):
+        dw_copy(2, b).wait_send()
+        for q in (0, 1):
+            @pl.when(outer)
+            def _():
+                dw_copy(q, b).wait_send()
+
+            @pl.when(inner)
+            def _():
+                dw_copy(3 + q, b).wait_send()
 
 
 def local(pass_ids, store, queries, gate_pre, w_query, w_gate, w_key, w_value, d_mem):
@@ -1064,7 +1113,7 @@
     tok_pair = tok_rows // tp_n
     sto_pair = pass_rows // tp_n
     gathered_bytes = 2 * 2 * st_n * pass_rows * cols
-    if lax.axis_size("grp") == 2 and hi_n == 2 and passages % 2 == 0 and gathered_bytes <= 8 << 20:
+    if lax.axis_size("grp") == 2 and hi_n == 2 and st_n == 4 and passages % 2 == 0 and gathered_bytes <= 8 << 20:
         half_pass = passages // 2
         n_some = half_pass // tile_of(half_pass, 2)
         d_tokens, d_store, d_wkey = pl.pallas_call(
@@ -1098,8 +1147,8 @@
                 V((pass_rows, pair), BF),
                 V((tp_n, sto_pair, pair), BF),
                 V((model, cols), BF),
-                V((st_n, share, cols), BF),
-                V((st_n, share, cols), BF),
+                V((2, share, cols), BF),
+                V((2, share, cols), BF),
                 V((tp_n, tok_pair, model), BF),
                 V((hi_n, tok_pair, model), BF),
                 V((hi_n, tok_pair, model), BF),
@@ -1118,8 +1167,8 @@
                 DMA((5, tp_n)),
                 DMA((2, tp_n)),
                 DMA((2, tp_n)),
-                DMA((2, st_n, 2)),
-                DMA((2, st_n, 2)),
+                DMA((5, 2)),
+                DMA((5, 2)),
             ],
             compiler_params=pltpu.CompilerParams(
                 collective_id=0, has_side_effects=True, vmem_limit_bytes=67043328

time: 151 us -> 127 us (0.84)
  Pallas kernels: 141 us -> 118 us
    pallas_call x1, Pallas kernels: 141 us -> 118 us  [local(): pl.pallas_call(functools.partial(gathered_kernel, st_n, tp_n, depth, pass...]
where the time goes in v2:
time: 127 us; the launch traced here: 126 us
  Pallas kernels  118 us (93%)
  local copies, waits for them, and re-layouts  6.25 us (5%)
  other arithmetic  1.74 us (1%)
    pallas_call x1, Pallas kernels, local(): pl.pallas_call(functools.partial(gathered_kernel, st_n, tp_n, depth, pass...  118 us
    unnamed x12, local copies, waits for them, and re-layouts  5.76 us

profile of v2, /device:TPU:1, one launch (start us, length us, event | category | flops | bytes accessed | tf_op | source)
XLA Modules:
  0.0 126.5 jit_solution(16894468323072132471)
XLA Ops:
  0.6 0.0 copy-start.3
  0.7 0.1 pad.7.clone
  0.7 0.6 copy-done.3
  1.3 0.1 copy.15
  1.4 0.1 reshape.230.ids_ref
  1.5 0.0 copy-start.2
  1.5 0.5 copy-done.2
  2.0 0.2 convert_reduce_fusion
  2.2 0.8 fusion.1
  3.0 0.1 broadcast_in_dim.51
  3.1 0.1 lt.50
  3.2 0.1 broadcast_in_dim.53
  3.3 0.1 mul.19
  3.4 0.7 add_add_fusion.ask_ref
  4.1 117.8 %shard_map.112 = (bf16[256,2048]{1,0:T(8,128)(2,1)}, bf16[256,2048]{1,0:T(8,128)(2,1)}, f32[512,256]{1,0:T(8,128)}) custom-call(s32[32]{0:T(128)} %copy-done.2, s32[4,8]{1,0:T(4,128)} %get-tuple-element.10.req_ref, s32[4,8,512]{2,1,0:T(8,128)} %add_add_fusion.ask_ref, bf16[1024,512]{1,0:T(8,128)(2,1)} %bitcast.2, bf16[1024,256]{1,0:T(8,128)(2,1)} %q_hbm.1, ...), custom_call_target="tpu_custom_call" | custom-call | tf_op jit(solution)/shard_map/pallas_call | solution.py:1119
  121.9 0.0 copy-start
  121.9 2.4 %copy.20 = bf16[256,2048]{1,0:T(8,128)(2,1)} copy(bf16[256,2048]{1,0:T(8,128)(2,1)} %get-tuple-element.18) | data formatting | bytes 2097152
  124.3 0.0 copy-done
  124.3 0.0 copy-start.1
  124.3 1.0 copy.21
  125.2 0.4 copy-done.1
  125.7 0.8 copy.22
  (10 shorter events, 0.1 us)
Async XLA Ops:
  0.6 0.7 copy-start.3
  1.5 0.5 copy-start.2
  121.9 2.4 %copy-start = (bf16[256,2048]{1,0:T(8,128)(2,1)S(1)}, bf16[256,2048]{1,0:T(8,128)(2,1)}, u32[]{:S(2)}) copy-start(bf16[256,2048]{1,0:T(8,128)(2,1)} %get-tuple-element.7) | copy-start | bytes 3145732
  124.3 1.4 %copy-start.1 = (f32[512,256]{1,0:T(8,128)S(1)}, f32[512,256]{1,0:T(8,128)}, u32[]{:S(2)}) copy-start(f32[512,256]{1,0:T(8,128)} %get-tuple-element.20) | copy-start | bytes 1572868

commit v3 on v2

--- a/solution.py
+++ b/solution.py
@@ -431,7 +431,7 @@
     st_n, tp_n, depth, pass_len,
     ids_ref, req_ref, ask_ref, store_ref, q_hbm, g_hbm, wq_hbm, wg_hbm, wk_hbm, wv_hbm, m_hbm,
     tok_out, store_out, wkey_out,
-    rows, wall, wqg, q_v, g_v, m_v, acc, vterm, k_all, v_all, ask_in, ret, prob_v, kvb, reqg, gboth, arr,
+    rows, wall, wqg, q_v, g_v, m_v, acc, terms, k_all, v_all, ask_in, ret, prob_v, kvb, reqg, gboth, arr,
     hot, plow, sums, dwp, dwc, dwf, tp_part, tp_pair, tp_recv,
     lsem, gs, gr, fs, fr, zs, zr, ps, pr, xs, xr, ws, wr, ss, sr, us, ur,
 ):
@@ -461,8 +461,8 @@
         copy.start()
         return copy
 
+    own_rows = local(0, store_ref, rows.at[tp])
     loads_kv = [
-        local(0, store_ref, rows.at[tp]),
         local(1, wk_hbm, wall.at[tp, :, pl.ds(0, cols)]),
         local(2, wv_hbm, wall.at[tp, :, pl.ds(cols, cols)]),
     ]
@@ -496,22 +496,21 @@
 
     def g_copy(way, i, t, source, peer, slot):
         r = pl.ds(first_row(i), some_rows)
-        src = store_ref.at[r] if source is None else rows.at[source, r]
-        return remote(src, rows.at[t, r], gs.at[way, slot, i], gr.at[t, i], peer)
+        return remote(rows.at[source, r], rows.at[t, r], gs.at[way, slot, i], gr.at[t, i], peer)
 
     def across(d, i):
         h = (hi + d) % hi_n
-        return g_copy(0, i, tp, None, {"tp": h * 2 + lo}, h)
+        return g_copy(0, i, tp, tp, {"tp": h * 2 + lo}, h)
 
     def beside(i):
-        return g_copy(1, i, tp, None, mate, hi)
+        return g_copy(1, i, tp, tp, mate, hi)
 
     def onward(d, i):
         h = (hi + d) % hi_n
         return g_copy(2, i, h * 2 + lo, h * 2 + lo, mate, h)
 
     def g_wait(t, i):
-        g_copy(1, i, t, None, mate, hi).wait_recv()
+        g_copy(1, i, t, t, mate, hi).wait_recv()
 
     def rows_send(i, c):
         for d in range(1, hi_n):
@@ -519,6 +518,7 @@
         beside(i).start()
         return c
 
+    own_rows.wait()
     lax.fori_loop(0, 2 * n_some, rows_send, 0)
 
     upper = st >= st_n // 2
@@ -543,29 +543,31 @@
     lax.fori_loop(1, st_n, ask_send, 0)
     ask_in[st] = ask_ref[st]
 
-    def project(i):
+    def project(i, send):
         r = pl.ds(first_row(i), some_rows)
 
-        def term(t):
-            w = wall[tp, pl.ds(pl.multiple_of(t * chunk, chunk), chunk), :]
-            return dot(rows[t, r], w)
+        def term(t, span):
+            return dot(rows[t, r], wall[tp, pl.ds(pl.multiple_of(t * chunk, chunk), chunk), span])
 
         for d in range(1, hi_n):
             g_wait(((hi + d) % hi_n) * 2 + lo, i)
             onward(d, i).start()
         g_wait(mate_t, i)
-        total = term(tp) + term(mate_t)
-        for d in range(1, hi_n):
-            total = total + term(((hi + d) % hi_n) * 2 + lo)
-        for d in range(1, hi_n):
-            t = ((hi + d) % hi_n) * 2 + 1 - lo
+        near = [tp, mate_t] + [((hi + d) % hi_n) * 2 + lo for d in range(1, hi_n)]
+        late = [((hi + d) % hi_n) * 2 + 1 - lo for d in range(1, hi_n)]
+        total = sum(term(t, key_cols) for t in near[1:]) + term(near[0], key_cols)
+        for t in late:
             g_wait(t, i)
-            total = total + term(t)
+            total = total + term(t, key_cols)
         low = total.astype(BF)
         first = st * passages + first_row(i) // pass_len
         for p in range(some):
-            k_all[first + p] = low[p * pass_len : (p + 1) * pass_len, key_cols]
-            v_all[first + p] = low[p * pass_len : (p + 1) * pass_len, value_cols]
+            k_all[first + p] = low[p * pass_len : (p + 1) * pass_len]
+        send()
+        total = sum(term(t, value_cols) for t in near + late)
+        low = total.astype(BF)
+        for p in range(some):
+            v_all[first + p] = low[p * pass_len : (p + 1) * pass_len]
 
     def part_of_all(kind, o, c, side):
         ref = k_all if kind == 0 else v_all
@@ -633,8 +635,7 @@
         copy.wait()
 
     def early_step(i, c):
-        project(i)
-        own_send(0, i)
+        project(i, lambda: own_send(0, i))
 
         @pl.when(i > 0)
         def _():
@@ -649,23 +650,35 @@
         own_send(1, i, outward=False)
         return c
 
+    lax.fori_loop(0, n_some, inward_send, 0)
+
+    def second_step(i, c):
+        relay(0, 2, i)
+        return c
+
     def outward_send(i, c):
         own_send(1, i, inward=False)
         return c
 
-    lax.fori_loop(0, n_some, inward_send, 0)
+    lax.fori_loop(0, n_some, second_step, 0)
+    lax.fori_loop(0, n_some, outward_send, 0)
 
     def late_step(i, c):
-        project(n_some + i)
-        relay(0, 2, i)
-        return c
-
-    lax.fori_loop(0, n_some, late_step, 0)
-    lax.fori_loop(0, n_some, outward_send, 0)
-
-    w_half = model // 2
-    w_mine = pl.ds(pl.multiple_of(grp * w_half, w_half), w_half)
-    w_other = pl.ds(pl.multiple_of((1 - grp) * w_half, w_half), w_half)
+        project(n_some + i, lambda: None)
+
+        @pl.when(edge)
+        def _():
+            relay(0, 3, i)
+
+        @pl.when(jnp.logical_not(edge))
+        def _():
+            relay(1, 1, i)
+
+        return c
+
+    w_part = model // 2
+    w_mine = pl.ds(pl.multiple_of(grp * w_part, w_part), w_part)
+    w_other = pl.ds(pl.multiple_of((1 - grp) * w_part, w_part), w_part)
 
     def w_across(d):
         h = (hi + d) % hi_n
@@ -689,7 +702,6 @@
 
     for d in range(1, hi_n):
         w_across(d).start()
-    w_beside.start()
 
     def relay_rest(kind, first, last):
         def step(i, c):
@@ -699,9 +711,10 @@
         lax.fori_loop(first, last, step, 0)
 
     relays = (st_n - 1) * n_some
-    ahead = jnp.where((st > 0) & (st < st_n - 1), n_some, 0)
-    relay_rest(1, 0, ahead)
-    relay_rest(0, 2 * n_some, relays)
+    edge = (st == 0) | (st == st_n - 1)
+    lax.fori_loop(0, n_some, late_step, 0)
+    w_beside.start()
+    relay_rest(1, 0, jnp.where(edge, n_some // 2, 0))
     for copy in loads_q:
         copy.wait()
     twin_wait(0)
@@ -728,11 +741,13 @@
             for j in range(PB):
                 reqg[b * PB + j, :, vs] = value_grad[j * pass_len : (j + 1) * pass_len]
 
-        i = ahead + b
-
-        @pl.when(i < relays)
+        @pl.when((b < n_some) & jnp.logical_not(edge))
         def _():
-            relay(1, 1 + i // n_some, i % n_some)
+            relay(1, 2, b)
+
+        @pl.when((b < n_some) & edge & (b % 2 == 1))
+        def _():
+            relay(1, 1, n_some // 2 + b // 2)
 
         return c
 
@@ -744,21 +759,27 @@
     def back_copy(phase, part, peer):
         return z_copy(phase, half(ret, peer, part), half(arr, st, part), peer)
 
-    def give_back(phase, part, span):
+    def give_back(phase, part, span, order, first, last):
         def send(d, c):
-            peer = far_peer(d)
+            peer = order(d)
             for k in range(depth):
                 ret[peer, k, :, span] = reqg[req_ref[peer, k]][:, span]
             back_copy(phase, part, peer).start()
             return c
 
-        lax.fori_loop(1, st_n, send, 0)
+        lax.fori_loop(first, last, send, 0)
+
+    def keep_own(span):
         for k in range(depth):
             arr[st, k, :, span] = reqg[req_ref[st, k]][:, span]
 
+    def near_peer(d):
+        return far_peer(st_n - d)
+
     ks, vs_all = pl.ds(0, cols), pl.ds(cols, cols)
-    give_back(1, vs_all, value_cols)
-    relay_rest(1, jnp.minimum(ahead + blocks, relays), relays)
+    give_back(1, vs_all, value_cols, near_peer, 1, jnp.where(edge, st_n, st_n - 1))
+    keep_own(value_cols)
+    relay_rest(1, jnp.where(edge, n_some, 2 * n_some), relays)
     twin_wait(1)
 
     def block_step(b, c):
@@ -788,40 +809,39 @@
         return c
 
     lax.fori_loop(0, blocks, block_step, 0)
-    give_back(2, ks, key_cols)
+    give_back(2, ks, key_cols, far_peer, 1, st_n)
+    keep_own(key_cols)
+
+    n_tile = tile_of(model, 512)
+
+    def expand(t):
+        a = gboth[pl.ds(pl.multiple_of(t * tok_pair, tok_pair), tok_pair), :]
+
+        def step(i, c):
+            n = pl.ds(pl.multiple_of(i * n_tile, n_tile), n_tile)
+            tp_part[t, :, n] = dot(a, wqg[n, :], NT).astype(BF)
+            return c
+
+        lax.fori_loop(0, model // n_tile, step, 0)
+
+    def pair_copy(h):
+        return remote(tp_part.at[h * 2 + 1 - lo], tp_pair.at[h], ps.at[h], pr.at[h], mate)
+
+    def cross(h):
+        return remote(
+            tp_part.at[h * 2 + lo], tp_recv.at[hi], xs.at[h], xr.at[hi], {"tp": h * 2 + lo}
+        )
 
     for d in range(1, hi_n):
         w_wait(0, ((hi + d) % hi_n) * 2 + lo, w_mine)
         w_twin(d).start()
         w_onward(d, 0).start()
-
-    n_tile = tile_of(model, 512)
-
-    def expand(t):
-        a = gboth[pl.ds(pl.multiple_of(t * tok_pair, tok_pair), tok_pair), :]
-
-        def step(i, c):
-            n = pl.ds(pl.multiple_of(i * n_tile, n_tile), n_tile)
-            tp_part[t, :, n] = dot(a, wqg[n, :], NT).astype(BF)
-            return c
-
-        lax.fori_loop(0, model // n_tile, step, 0)
-
-    def pair_copy(h):
-        return remote(tp_part.at[h * 2 + 1 - lo], tp_pair.at[h], ps.at[h], pr.at[h], mate)
-
-    def cross(h):
-        return remote(
-            tp_part.at[h * 2 + lo], tp_recv.at[hi], xs.at[h], xr.at[hi], {"tp": h * 2 + lo}
-        )
 
     tok_pair = tok_rows // tp_n
     for d in range(1, hi_n + 1):
         h = (hi + d) % hi_n
         expand(h * 2 + 1 - lo)
         pair_copy(h).start()
-    for d in range(1, hi_n + 1):
-        h = (hi + d) % hi_n
         expand(h * 2 + lo)
         pair_copy(h).wait_recv()
         if d < hi_n:
@@ -846,11 +866,11 @@
 
     lax.fori_loop(0, st_n, hot_step, 0)
 
-    def gather_sums(o, span, first):
+    def gather_sums(kind, o, span, first):
         def step(i, c):
             r = pl.ds(pl.multiple_of(i * m_tile, m_tile), m_tile)
             part = dot(hot[o, r, :], arr[o, :, :, span].reshape(hot_cols, cols))
-            acc[r, :] = part if first else acc[r, :] + part
+            acc[kind, r, :] = part if first else acc[kind, r, :] + part
             return c
 
         lax.fori_loop(0, pass_rows // m_tile, step, 0)
@@ -866,33 +886,41 @@
         dst = sums.at[t, :, part]
         remote(dst, dst, ss.at[kind, t], sr.at[kind, t], mate).wait_recv()
 
-    def collect(phase, kind, part, span):
-        gather_sums(st, span, True)
-
-        def grad_wait(d, c):
-            peer = (st + d) % st_n
-            z_wait(phase, half(ret, peer, part), half(arr, peer, part), peer)
-            gather_sums(peer, span, False)
-            return c
-
-        lax.fori_loop(1, st_n, grad_wait, 0)
-        plow[:, span] = acc[...].astype(BF)
+    def grads_of(kind, peer):
+        phase, part, span = (2, ks, key_cols) if kind == 0 else (1, vs_all, value_cols)
+        z_wait(phase, half(ret, peer, part), half(arr, peer, part), peer)
+        gather_sums(kind, peer, span, False)
+
+    def sums_send(kind):
+        part, span = (ks, key_cols) if kind == 0 else (vs_all, value_cols)
+        plow[:, span] = acc[kind].astype(BF)
         for d in range(1, tp_n):
             sums_copy(kind, part, d).start()
         sums[tp, :, span] = plow[pl.ds(pl.multiple_of(tp * sto_pair, sto_pair), sto_pair), span]
 
-    collect(1, 1, vs_all, value_cols)
-
-    collect(2, 0, ks, key_cols)
+    beyond = jnp.where(lower, st_n - 1, 0)
+    middle = jnp.where(lower, st_n // 2, st_n // 2 - 1)
+    beside_st = st + 1 - 2 * (st % 2)
+    outer = edge
+    inner = jnp.logical_not(outer)
+    gather_sums(1, st, value_cols, True)
+    gather_sums(0, st, key_cols, True)
+    grads_of(1, beside_st)
+    grads_of(1, jnp.where(outer, beyond, middle))
+
+    grads_of(0, middle)
+
+    @pl.when(inner)
+    def _():
+        give_back(1, vs_all, value_cols, near_peer, st_n - 1, st_n)
+
+    grads_of(0, beyond)
+    grads_of(0, beside_st)
+    sums_send(0)
 
     share = model // st_n
     bits = 2
     bit = share // bits
-    beyond = jnp.where(lower, st_n - 1, 0)
-    middle = jnp.where(lower, st_n // 2, st_n // 2 - 1)
-    beside_st = st + 1 - 2 * (st % 2)
-    outer = (st == 0) | (st == st_n - 1)
-    inner = jnp.logical_not(outer)
 
     def dw_line(s, b):
         return pl.ds(pl.multiple_of(s * share + b * bit, bit), bit)
@@ -949,7 +977,8 @@
     lax.fori_loop(0, st_n, wkey_turn, 0)
 
     for d in range(1, hi_n):
-        w_wait(1, ((hi + d) % hi_n) * 2 + lo, w_other)
+        t = ((hi + d) % hi_n) * 2 + lo
+        w_wait(1, t, w_other)
         w_onward(d, 1).start()
     w_wait(4, mate_t, pl.ds(0, model))
     for d in range(1, hi_n):
@@ -968,23 +997,22 @@
 
         lax.fori_loop(0, model // n_tile, step, 0)
 
-    def keep_values(n, part):
-        vterm[:, n] = part
+    def keep_terms(n, part):
+        terms[:, n] = part
 
     def keep_store(n, part):
-        store_out[:, n] = (vterm[:, n] + part).astype(BF)
-
-    for d in range(1, tp_n):
-        sums_wait(1, vs_all, (tp + d) % tp_n)
-    store_terms(value_cols, keep_values)
+        store_out[:, n] = (terms[:, n] + part).astype(BF)
 
     @pl.when(inner)
     def _():
         dw_relay(0)
 
+    grads_of(1, jnp.where(outer, middle, beyond))
+    sums_send(1)
+
     for d in range(1, tp_n):
         sums_wait(0, ks, (tp + d) % tp_n)
-    store_terms(key_cols, keep_store)
+    store_terms(key_cols, keep_terms)
 
     for d in range(1, hi_n):
         h = (hi + d) % hi_n
@@ -999,6 +1027,10 @@
     @pl.when(inner)
     def _():
         dw_relay(1)
+
+    for d in range(1, tp_n):
+        sums_wait(1, vs_all, (tp + d) % tp_n)
+    store_terms(value_cols, keep_store)
 
     for b in range(bits):
         line = slice(b * bit, (b + 1) * bit)
@@ -1132,7 +1164,7 @@
                 V((tok_rows, cols), BF),
                 V((tok_rows, cols), BF),
                 V((tok_rows, cols), BF),
-                V((pass_rows, cols), F32),
+                V((2, pass_rows, cols), F32),
                 V((sto_pair, model), F32),
                 V((st_n * passages, pass_len, cols), BF),
                 V((st_n * passages, pass_len, cols), BF),

time: 127 us -> 121 us (0.953)
  Pallas kernels: 118 us -> 111 us
    pallas_call x1, Pallas kernels: 118 us -> 111 us  [local(): pl.pallas_call(functools.partial(gathered_kernel, st_n, tp_n, depth, pass...]
where the time goes in v3:
time: 121 us; the launch traced here: 120 us
  Pallas kernels  111 us (92%)
  local copies, waits for them, and re-layouts  6.25 us (5%)
  other arithmetic  1.74 us (1%)
    pallas_call x1, Pallas kernels, local(): pl.pallas_call(functools.partial(gathered_kernel, st_n, tp_n, depth, pass...  111 us
    unnamed x12, local copies, waits for them, and re-layouts  5.76 us

profile of v3, /device:TPU:1, one launch (start us, length us, event | category | flops | bytes accessed | tf_op | source)
XLA Modules:
  0.0 119.9 jit_solution(8720286761154578496)
XLA Ops:
  0.6 0.0 copy-start.3
  0.7 0.1 pad.7.clone
  0.7 0.6 copy-done.3
  1.3 0.1 copy.15
  1.4 0.1 reshape.230.ids_ref
  1.5 0.0 copy-start.2
  1.5 0.5 copy-done.2
  2.0 0.2 convert_reduce_fusion
  2.2 0.8 fusion.1
  3.0 0.1 broadcast_in_dim.51
  3.1 0.1 lt.50
  3.2 0.1 broadcast_in_dim.53
  3.3 0.1 mul.19
  3.4 0.7 add_add_fusion.ask_ref
  4.1 111.2 %shard_map.112 = (bf16[256,2048]{1,0:T(8,128)(2,1)}, bf16[256,2048]{1,0:T(8,128)(2,1)}, f32[512,256]{1,0:T(8,128)}) custom-call(s32[32]{0:T(128)} %copy-done.2, s32[4,8]{1,0:T(4,128)} %get-tuple-element.10.req_ref, s32[4,8,512]{2,1,0:T(8,128)} %add_add_fusion.ask_ref, bf16[1024,512]{1,0:T(8,128)(2,1)} %bitcast.2, bf16[1024,256]{1,0:T(8,128)(2,1)} %q_hbm.1, ...), custom_call_target="tpu_custom_call" | custom-call | tf_op jit(solution)/shard_map/pallas_call | solution.py:1151
  115.3 0.0 copy-start
  115.3 2.4 %copy.20 = bf16[256,2048]{1,0:T(8,128)(2,1)} copy(bf16[256,2048]{1,0:T(8,128)(2,1)} %get-tuple-element.18) | data formatting | bytes 2097152
  117.7 0.0 copy-done
  117.7 0.0 copy-start.1
  117.7 1.0 copy.21
  118.7 0.4 copy-done.1
  119.1 0.8 copy.22
  (10 shorter events, 0.1 us)
Async XLA Ops:
  0.6 0.7 copy-start.3
  1.5 0.5 copy-start.2
  115.3 2.4 %copy-start = (bf16[256,2048]{1,0:T(8,128)(2,1)S(1)}, bf16[256,2048]{1,0:T(8,128)(2,1)}, u32[]{:S(2)}) copy-start(bf16[256,2048]{1,0:T(8,128)(2,1)} %get-tuple-element.7) | copy-start | bytes 3145732
  117.7 1.4 %copy-start.1 = (f32[512,256]{1,0:T(8,128)S(1)}, f32[512,256]{1,0:T(8,128)}, u32[]{:S(2)}) copy-start(f32[512,256]{1,0:T(8,128)} %get-tuple-element.20) | copy-start | bytes 1572868

commit v4 on v3

--- a/solution.py
+++ b/solution.py
@@ -429,9 +429,9 @@
 
 def gathered_kernel(
     st_n, tp_n, depth, pass_len,
-    ids_ref, req_ref, ask_ref, store_ref, q_hbm, g_hbm, wq_hbm, wg_hbm, wk_hbm, wv_hbm, m_hbm,
+    ids_ref, store_ref, q_hbm, g_hbm, wq_hbm, wg_hbm, wk_hbm, wv_hbm, m_hbm,
     tok_out, store_out, wkey_out,
-    rows, wall, wqg, q_v, g_v, m_v, acc, terms, k_all, v_all, ask_in, ret, prob_v, kvb, reqg, gboth, arr,
+    rows, wall, wqg, q_v, g_v, m_v, acc, terms, k_all, v_all, ask_v, ask_in, order_v, req_ref, gated, slope, ret, prob_v, kvb, reqg, gboth, arr,
     hot, plow, sums, dwp, dwc, dwf, tp_part, tp_pair, tp_recv,
     lsem, gs, gr, fs, fr, zs, zr, ps, pr, xs, xr, ws, wr, ss, sr, us, ur,
 ):
@@ -488,6 +488,34 @@
             barrier, inc=1, device_id={"tp": (tp + d) % tp_n}, device_id_type=MESH
         )
     pl.semaphore_signal(barrier, inc=1, device_id=twin, device_id_type=MESH)
+
+    def plan(wide):
+        line = lax.broadcasted_iota(jnp.int32, (8, wide), 0)
+        return line, lax.broadcasted_iota(jnp.int32, (8, wide), 1)
+
+    width = ask_v.shape[2]
+    line, lane = plan(width)
+    slot, place = lane // pass_len, lane % pass_len
+    short_line, short_lane = plan(order_v.shape[1])
+    target = jnp.full((8, width), -1, jnp.int32)
+    order = jnp.zeros(order_v.shape, jnp.int32)
+    taken = [jnp.int32(0)] * st_n
+    for j in range(PB):
+        for n in range(blocks):
+            i = ids_ref[j, n]
+            owner = lax.div(i, jnp.int32(passages))
+            within = i - owner * passages
+            rank = sum(jnp.where(owner == o, taken[o], 0) for o in range(st_n))
+            taken = [taken[o] + jnp.where(owner == o, 1, 0) for o in range(st_n)]
+            target = jnp.where(
+                (line == owner) & (slot == rank), within * pass_len + place, target
+            )
+            order = jnp.where(
+                (short_line == owner) & (short_lane == rank), j * blocks + n, order
+            )
+    order_v[...] = order
+    for o in range(st_n):
+        ask_v[o] = jnp.broadcast_to(target[o : o + 1], (8, width))
     pl.semaphore_wait(barrier, st_n + tp_n - 1)
 
     def first_row(i):
@@ -537,11 +565,12 @@
 
     def ask_send(d, c):
         peer = (st + d) % st_n
-        z_copy(0, ask_ref.at[peer], ask_in.at[st], peer).start()
+        z_copy(0, ask_v.at[peer], ask_in.at[st], peer).start()
         return c
 
     lax.fori_loop(1, st_n, ask_send, 0)
-    ask_in[st] = ask_ref[st]
+    ask_in[st] = ask_v[st]
+    order_copy = local(8, order_v, req_ref)
 
     def project(i, send):
         r = pl.ds(first_row(i), some_rows)
@@ -582,6 +611,7 @@
         return remote(part, part, fs.at[kind, o, c, 2], fr.at[kind, o, c, 1], twin)
 
     lower = st < st_n // 2
+    edge = (st == 0) | (st == st_n - 1)
 
     def own_copies(kind, c, act, inward=True, outward=True):
         ways = ((0, st + 1, lower), (1, st - 1, jnp.logical_not(lower)))
@@ -631,8 +661,18 @@
 
         lax.fori_loop(0, (st_n - 1) * n_some, step, 0)
 
-    for copy in loads_kv:
+    for copy in loads_kv + loads_q[:3]:
         copy.wait()
+
+    gate_rows = tok_rows // n_some
+
+    def gates(i):
+        r = pl.ds(pl.multiple_of(i * gate_rows, gate_rows), gate_rows)
+        gate = g_v[r, :].astype(F32)
+        grad = m_v[r, :].astype(F32)
+        sig = 1.0 / (1.0 + jnp.exp(-gate))
+        gated[r, :] = (gate * sig * grad).astype(BF)
+        slope[r, :] = grad * (sig * (1.0 + gate * (1.0 - sig)))
 
     def early_step(i, c):
         project(i, lambda: own_send(0, i))
@@ -641,6 +681,11 @@
         def _():
             relay(0, 1, i - 1)
 
+        @pl.when(edge | (i == 0))
+        def _():
+            own_send(1, i, outward=False)
+
+        gates(i)
         return c
 
     lax.fori_loop(0, n_some, early_step, 0)
@@ -650,7 +695,7 @@
         own_send(1, i, outward=False)
         return c
 
-    lax.fori_loop(0, n_some, inward_send, 0)
+    lax.fori_loop(jnp.where(edge, n_some, 1), n_some, inward_send, 0)
 
     def second_step(i, c):
         relay(0, 2, i)
@@ -711,47 +756,48 @@
         lax.fori_loop(first, last, step, 0)
 
     relays = (st_n - 1) * n_some
-    edge = (st == 0) | (st == st_n - 1)
     lax.fori_loop(0, n_some, late_step, 0)
     w_beside.start()
-    relay_rest(1, 0, jnp.where(edge, n_some // 2, 0))
-    for copy in loads_q:
+    relay_rest(1, 0, jnp.where(edge, n_some, 0))
+    for copy in loads_q[3:]:
         copy.wait()
+    order_copy.wait()
     twin_wait(0)
     scale = HD ** (-0.5)
 
-    def fill(ref, span, b):
+    def fill(n, ref, span, b):
         for j in range(PB):
-            kvb[j * pass_len : (j + 1) * pass_len, span] = ref[ids_ref[b * PB + j]]
-
-    def probs_step(b, c):
-        r = pl.ds(pl.multiple_of(b * BLK, BLK), BLK)
-        fill(k_all, key_cols, b)
+            kvb[n, j * pass_len : (j + 1) * pass_len, span] = ref[ids_ref[j, b]]
+
+    pairs = range(2)
+
+    def block_rows(b):
+        return pl.ds(pl.multiple_of(b * BLK, BLK), BLK)
+
+    def probs_step(i, c):
+        for n in pairs:
+            fill(n, k_all, key_cols, 2 * i + n)
         for head in range(heads):
             hs = slice(head * HD, (head + 1) * HD)
             vs = slice(cols + head * HD, cols + (head + 1) * HD)
-            gate = g_v[r, hs].astype(F32)
-            scores = dot(q_v[r, hs], kvb[:, hs], NT) * scale
-            shifted = jnp.exp(scores - jnp.max(scores, axis=-1, keepdims=True))
-            prob = shifted / jnp.sum(shifted, axis=-1, keepdims=True)
-            prob_v[head, r, :] = prob
-            sig = 1.0 / (1.0 + jnp.exp(-gate))
-            att_grad = (gate * sig * m_v[r, hs].astype(F32)).astype(BF)
-            value_grad = dot(prob.astype(BF), att_grad, TN).astype(BF)
-            for j in range(PB):
-                reqg[b * PB + j, :, vs] = value_grad[j * pass_len : (j + 1) * pass_len]
-
-        @pl.when((b < n_some) & jnp.logical_not(edge))
+            for n in pairs:
+                b = 2 * i + n
+                r = block_rows(b)
+                scores = dot(q_v[r, hs], kvb[n, :, hs], NT) * scale
+                shifted = jnp.exp(scores - jnp.max(scores, axis=-1, keepdims=True))
+                prob = shifted * (1.0 / jnp.sum(shifted, axis=-1, keepdims=True))
+                prob_v[head, r, :] = prob
+                value_grad = dot(prob.astype(BF), gated[r, hs], TN).astype(BF)
+                for j in range(PB):
+                    reqg[j * blocks + b, :, vs] = value_grad[j * pass_len : (j + 1) * pass_len]
+
+        @pl.when(i < n_some)
         def _():
-            relay(1, 2, b)
-
-        @pl.when((b < n_some) & edge & (b % 2 == 1))
-        def _():
-            relay(1, 1, n_some // 2 + b // 2)
-
-        return c
-
-    lax.fori_loop(0, blocks, probs_step, 0)
+            relay(1, 2, i)
+
+        return c
+
+    lax.fori_loop(0, blocks // 2, probs_step, 0)
 
     def half(ref, peer, part):
         return ref.at[peer, :, :, part]
@@ -777,49 +823,53 @@
         return far_peer(st_n - d)
 
     ks, vs_all = pl.ds(0, cols), pl.ds(cols, cols)
-    give_back(1, vs_all, value_cols, near_peer, 1, jnp.where(edge, st_n, st_n - 1))
+    def value_peer(d):
+        return jnp.where(edge, near_peer(d % (st_n - 1) + 1), near_peer(d))
+
+    give_back(
+        1, vs_all, value_cols, value_peer, 1, jnp.where(edge, st_n, st_n - 1)
+    )
     keep_own(value_cols)
-    relay_rest(1, jnp.where(edge, n_some, 2 * n_some), relays)
+    relay_rest(1, n_some + min(n_some, blocks // 2), relays)
     twin_wait(1)
 
-    def block_step(b, c):
-        r = pl.ds(pl.multiple_of(b * BLK, BLK), BLK)
-        fill(k_all, key_cols, b)
-        fill(v_all, value_cols, b)
+    def block_step(i, c):
+        for n in pairs:
+            fill(n, k_all, key_cols, 2 * i + n)
+            fill(n, v_all, value_cols, 2 * i + n)
         for head in range(heads):
             hs = slice(head * HD, (head + 1) * HD)
             vs = slice(cols + head * HD, cols + (head + 1) * HD)
-            q = q_v[r, hs]
-            key = kvb[:, hs]
-            value = kvb[:, vs]
-            gate = g_v[r, hs].astype(F32)
-            grad = m_v[r, hs].astype(F32)
-            prob = prob_v[head, r, :]
-            attended = dot(prob.astype(BF), value)
-            sig = 1.0 / (1.0 + jnp.exp(-gate))
-            att_grad = (gate * sig * grad).astype(BF)
-            gboth[r, vs] = (grad * attended * sig * (1.0 + gate * (1.0 - sig))).astype(BF)
-            prob_grad = dot(att_grad, value, NT)
-            inner = jnp.sum(prob * prob_grad, axis=-1, keepdims=True)
-            score_grad = (scale * prob * (prob_grad - inner)).astype(BF)
-            gboth[r, hs] = dot(score_grad, key).astype(BF)
-            key_grad = dot(score_grad, q, TN).astype(BF)
-            for j in range(PB):
-                reqg[b * PB + j, :, hs] = key_grad[j * pass_len : (j + 1) * pass_len]
-        return c
-
-    lax.fori_loop(0, blocks, block_step, 0)
+            for n in pairs:
+                b = 2 * i + n
+                r = block_rows(b)
+                value = kvb[n, :, vs]
+                prob = prob_v[head, r, :]
+                prob_grad = dot(gated[r, hs], value, NT)
+                inner = jnp.sum(prob * prob_grad, axis=-1, keepdims=True)
+                score_grad = (scale * prob * (prob_grad - inner)).astype(BF)
+                key_grad = dot(score_grad, q_v[r, hs], TN).astype(BF)
+                for j in range(PB):
+                    reqg[j * blocks + b, :, hs] = key_grad[j * pass_len : (j + 1) * pass_len]
+                gboth[r, hs] = dot(score_grad, kvb[n, :, hs]).astype(BF)
+                attended = dot(prob.astype(BF), value)
+                gboth[r, vs] = (attended * slope[r, hs]).astype(BF)
+        return c
+
+    lax.fori_loop(0, blocks // 2, block_step, 0)
     give_back(2, ks, key_cols, far_peer, 1, st_n)
     keep_own(key_cols)
 
     n_tile = tile_of(model, 512)
 
-    def expand(t):
-        a = gboth[pl.ds(pl.multiple_of(t * tok_pair, tok_pair), tok_pair), :]
+    def expand(h):
+        a = gboth[pl.ds(pl.multiple_of(h * 2 * tok_pair, tok_pair), 2 * tok_pair), :]
 
         def step(i, c):
             n = pl.ds(pl.multiple_of(i * n_tile, n_tile), n_tile)
-            tp_part[t, :, n] = dot(a, wqg[n, :], NT).astype(BF)
+            part = dot(a, wqg[n, :], NT).astype(BF)
+            tp_part[h * 2, :, n] = part[:tok_pair]
+            tp_part[h * 2 + 1, :, n] = part[tok_pair:]
             return c
 
         lax.fori_loop(0, model // n_tile, step, 0)
@@ -840,17 +890,17 @@
     tok_pair = tok_rows // tp_n
     for d in range(1, hi_n + 1):
         h = (hi + d) % hi_n
-        expand(h * 2 + 1 - lo)
+        expand(h)
         pair_copy(h).start()
-        expand(h * 2 + lo)
+    for d in range(1, hi_n):
+        h = (hi + d) % hi_n
         pair_copy(h).wait_recv()
-        if d < hi_n:
-            tp_part[h * 2 + lo] = (tp_part[h * 2 + lo].astype(F32) + tp_pair[h].astype(F32)).astype(BF)
-            cross(h).start()
+        tp_part[h * 2 + lo] = (tp_part[h * 2 + lo].astype(F32) + tp_pair[h].astype(F32)).astype(BF)
+        cross(h).start()
 
     def ask_wait(d, c):
         peer = (st + d) % st_n
-        z_wait(0, ask_ref.at[peer], ask_in.at[peer], peer)
+        z_wait(0, ask_v.at[peer], ask_in.at[peer], peer)
         return c
 
     lax.fori_loop(1, st_n, ask_wait, 0)
@@ -976,6 +1026,10 @@
 
     lax.fori_loop(0, st_n, wkey_turn, 0)
 
+    @pl.when(inner)
+    def _():
+        dw_relay(0)
+
     for d in range(1, hi_n):
         t = ((hi + d) % hi_n) * 2 + lo
         w_wait(1, t, w_other)
@@ -1003,10 +1057,6 @@
     def keep_store(n, part):
         store_out[:, n] = (terms[:, n] + part).astype(BF)
 
-    @pl.when(inner)
-    def _():
-        dw_relay(0)
-
     grads_of(1, jnp.where(outer, middle, beyond))
     sums_send(1)
 
@@ -1014,6 +1064,7 @@
         sums_wait(0, ks, (tp + d) % tp_n)
     store_terms(key_cols, keep_terms)
 
+    pair_copy(hi).wait_recv()
     for d in range(1, hi_n):
         h = (hi + d) % hi_n
         remote(
@@ -1074,7 +1125,7 @@
 
     def drain(d, c):
         peer = (st + d) % st_n
-        z_copy(0, ask_ref.at[peer], ask_in.at[st], peer).wait_send()
+        z_copy(0, ask_v.at[peer], ask_in.at[st], peer).wait_send()
         back_copy(1, vs_all, peer).wait_send()
         back_copy(2, ks, peer).wait_send()
         return c
@@ -1112,6 +1163,88 @@
     depth = max(2, requests // st_n)
     pass_rows = passages * pass_len
     share = model // st_n
+
+    vmem = pl.BlockSpec(memory_space=pltpu.VMEM)
+    smem = pl.BlockSpec(memory_space=pltpu.SMEM)
+    hbm = pl.BlockSpec(memory_space=pl.ANY)
+    V = pltpu.VMEM
+    DMA = pltpu.SemaphoreType.DMA
+    pair = 2 * cols
+    tok_pair = tok_rows // tp_n
+    sto_pair = pass_rows // tp_n
+    hot_cols = depth * pass_len
+    width = -(-hot_cols // 128) * 128
+    gathered_bytes = 2 * 2 * st_n * pass_rows * cols
+    if lax.axis_size("grp") == 2 and hi_n == 2 and st_n == 4 and passages % 2 == 0 and gathered_bytes <= 8 << 20:
+        half_pass = passages // 2
+        n_some = half_pass // tile_of(half_pass, 2)
+        d_tokens, d_store, d_wkey = pl.pallas_call(
+            functools.partial(gathered_kernel, st_n, tp_n, depth, pass_len),
+            out_shape=(
+                jax.ShapeDtypeStruct((tok_pair, model), BF),
+                jax.ShapeDtypeStruct((sto_pair, model), BF),
+                jax.ShapeDtypeStruct((share, cols), F32),
+            ),
+            in_specs=[smem] + [hbm] * 8,
+            out_specs=(vmem, vmem, vmem),
+            scratch_shapes=[
+                V((tp_n, pass_rows, chunk), BF),
+                V((tp_n, model, pair), BF),
+                V((model, pair), BF),
+                V((tok_rows, cols), BF),
+                V((tok_rows, cols), BF),
+                V((tok_rows, cols), BF),
+                V((2, pass_rows, cols), F32),
+                V((sto_pair, model), F32),
+                V((st_n * passages, pass_len, cols), BF),
+                V((st_n * passages, pass_len, cols), BF),
+                V((st_n, 8, width), jnp.int32),
+                V((st_n, 8, width), jnp.int32),
+                V((8, 128), jnp.int32),
+                pltpu.SMEM((8, 128), jnp.int32),
+                V((tok_rows, cols), BF),
+                V((tok_rows, cols), F32),
+                V((st_n, depth, pass_len, pair), BF),
+                V((cols // HD, tok_rows, PB * pass_len), F32),
+                V((2, PB * pass_len, pair), BF),
+                V((requests, pass_len, pair), BF),
+                V((tok_rows, pair), BF),
+                V((st_n, depth, pass_len, pair), BF),
+                V((st_n, pass_rows, hot_cols), BF),
+                V((pass_rows, pair), BF),
+                V((tp_n, sto_pair, pair), BF),
+                V((model, cols), BF),
+                V((2, share, cols), BF),
+                V((2, share, cols), BF),
+                V((tp_n, tok_pair, model), BF),
+                V((hi_n, tok_pair, model), BF),
+                V((hi_n, tok_pair, model), BF),
+                DMA((9,)),
+                DMA((3, hi_n, 2 * n_some)),
+                DMA((tp_n, 2 * n_some)),
+                DMA((2, st_n, n_some, 3)),
+                DMA((2, st_n, n_some, 2)),
+                DMA((3, st_n)),
+                DMA((3, st_n)),
+                DMA((hi_n,)),
+                DMA((hi_n,)),
+                DMA((hi_n,)),
+                DMA((hi_n,)),
+                DMA((5, hi_n)),
+                DMA((5, tp_n)),
+                DMA((2, tp_n)),
+                DMA((2, tp_n)),
+                DMA((5, 2)),
+                DMA((5, 2)),
+            ],
+            compiler_params=pltpu.CompilerParams(
+                collective_id=0, has_side_effects=True, vmem_limit_bytes=67043328
+            ),
+        )(
+            pass_ids.T, store.reshape(pass_rows, chunk),
+            queries, gate_pre, w_query, w_gate, w_key, w_value, d_mem,
+        )
+        return d_tokens, d_store.reshape(passages // tp_n, pass_len, model), d_wkey
 
     ids = pass_ids.reshape(-1)
     owners = ids // passages
@@ -1136,80 +1269,6 @@
         [target[:, None], flat[:, None], jnp.zeros((st_n, 6, width), jnp.int32)], axis=1
     )
 
-    vmem = pl.BlockSpec(memory_space=pltpu.VMEM)
-    smem = pl.BlockSpec(memory_space=pltpu.SMEM)
-    hbm = pl.BlockSpec(memory_space=pl.ANY)
-    V = pltpu.VMEM
-    DMA = pltpu.SemaphoreType.DMA
-    pair = 2 * cols
-    tok_pair = tok_rows // tp_n
-    sto_pair = pass_rows // tp_n
-    gathered_bytes = 2 * 2 * st_n * pass_rows * cols
-    if lax.axis_size("grp") == 2 and hi_n == 2 and st_n == 4 and passages % 2 == 0 and gathered_bytes <= 8 << 20:
-        half_pass = passages // 2
-        n_some = half_pass // tile_of(half_pass, 2)
-        d_tokens, d_store, d_wkey = pl.pallas_call(
-            functools.partial(gathered_kernel, st_n, tp_n, depth, pass_len),
-            out_shape=(
-                jax.ShapeDtypeStruct((tok_pair, model), BF),
-                jax.ShapeDtypeStruct((sto_pair, model), BF),
-                jax.ShapeDtypeStruct((share, cols), F32),
-            ),
-            in_specs=[smem, smem, vmem] + [hbm] * 8,
-            out_specs=(vmem, vmem, vmem),
-            scratch_shapes=[
-                V((tp_n, pass_rows, chunk), BF),
-                V((tp_n, model, pair), BF),
-                V((model, pair), BF),
-                V((tok_rows, cols), BF),
-                V((tok_rows, cols), BF),
-                V((tok_rows, cols), BF),
-                V((2, pass_rows, cols), F32),
-                V((sto_pair, model), F32),
-                V((st_n * passages, pass_len, cols), BF),
-                V((st_n * passages, pass_len, cols), BF),
-                V((st_n, 8, width), jnp.int32),
-                V((st_n, depth, pass_len, pair), BF),
-                V((cols // HD, tok_rows, PB * pass_len), F32),
-                V((PB * pass_len, pair), BF),
-                V((requests, pass_len, pair), BF),
-                V((tok_rows, pair), BF),
-                V((st_n, depth, pass_len, pair), BF),
-                V((st_n, pass_rows, hot_cols), BF),
-                V((pass_rows, pair), BF),
-                V((tp_n, sto_pair, pair), BF),
-                V((model, cols), BF),
-                V((2, share, cols), BF),
-                V((2, share, cols), BF),
-                V((tp_n, tok_pair, model), BF),
-                V((hi_n, tok_pair, model), BF),
-                V((hi_n, tok_pair, model), BF),
-                DMA((8,)),
-                DMA((3, hi_n, 2 * n_some)),
-                DMA((tp_n, 2 * n_some)),
-                DMA((2, st_n, n_some, 3)),
-                DMA((2, st_n, n_some, 2)),
-                DMA((3, st_n)),
-                DMA((3, st_n)),
-                DMA((hi_n,)),
-                DMA((hi_n,)),
-                DMA((hi_n,)),
-                DMA((hi_n,)),
-                DMA((5, hi_n)),
-                DMA((5, tp_n)),
-                DMA((2, tp_n)),
-                DMA((2, tp_n)),
-                DMA((5, 2)),
-                DMA((5, 2)),
-            ],
-            compiler_params=pltpu.CompilerParams(
-                collective_id=0, has_side_effects=True, vmem_limit_bytes=67043328
-            ),
-        )(
-            ids, req_of, ask, store.reshape(pass_rows, chunk),
-            queries, gate_pre, w_query, w_gate, w_key, w_value, d_mem,
-        )
-        return d_tokens, d_store.reshape(passages // tp_n, pass_len, model), d_wkey
     d_tokens, d_store, d_wkey = pl.pallas_call(
         functools.partial(kernel, st_n, tp_n, depth, pass_len),
         out_shape=(

time: 121 us -> 112 us (0.926)
  Pallas kernels: 111 us -> 107 us
  other arithmetic: 1.74 us -> 0 us
  local copies, waits for them, and re-layouts: 6.25 us -> 4.59 us
    pallas_call x1, Pallas kernels: 111 us -> 107 us  [local(): pl.pallas_call(functools.partial(gathered_kernel, st_n, tp_n, depth, pass...]
    unnamed x12 -> x7, local copies, waits for them, and re-layouts: 5.76 us -> 4.59 us
where the time goes in v4:
time: 112 us
  Pallas kernels  107 us (96%)
  local copies, waits for them, and re-layouts  4.59 us (4%)
    pallas_call x1, Pallas kernels, local(): pl.pallas_call(functools.partial(gathered_kernel, st_n, tp_n, depth, pass...  107 us
    unnamed x7, local copies, waits for them, and re-layouts  4.59 us

profile of v4, /device:TPU:1, one launch (start us, length us, event | category | flops | bytes accessed | tf_op | source)
XLA Modules:
  0.0 112.1 jit_solution(10618956356923732796)
XLA Ops:
  0.6 106.8 %shard_map.112 = (bf16[256,2048]{1,0:T(8,128)(2,1)}, bf16[256,2048]{1,0:T(8,128)(2,1)}, f32[512,256]{1,0:T(8,128)}) custom-call(s32[4,8]{1,0:T(4,128)} %bitcast.5, bf16[1024,512]{1,0:T(8,128)(2,1)} %bitcast.3, bf16[1024,256]{1,0:T(8,128)(2,1)} %q_hbm.1, bf16[1024,256]{1,0:T(8,128)(2,1)} %g_hbm.1, bf16[2048,256]{1,0:T(8,128)(2,1)} %wq_hbm.1, ...), custom_call_target="tpu_custom_call" | custom-call | tf_op jit(solution)/shard_map/pallas_call | solution.py:1181
  107.5 0.0 copy-start
  107.5 2.4 %copy.15 = bf16[256,2048]{1,0:T(8,128)(2,1)} copy(bf16[256,2048]{1,0:T(8,128)(2,1)} %get-tuple-element.12) | data formatting | bytes 2097152
  109.9 0.0 copy-done
  109.9 0.0 copy-start.1
  109.9 1.0 copy.16
  110.9 0.4 copy-done.1
  111.3 0.8 copy.17
Async XLA Ops:
  107.5 2.4 %copy-start = (bf16[256,2048]{1,0:T(8,128)(2,1)S(1)}, bf16[256,2048]{1,0:T(8,128)(2,1)}, u32[]{:S(2)}) copy-start(bf16[256,2048]{1,0:T(8,128)(2,1)} %get-tuple-element.7) | copy-start | bytes 3145732
  109.9 1.4 %copy-start.1 = (f32[512,256]{1,0:T(8,128)S(1)}, f32[512,256]{1,0:T(8,128)}, u32[]{:S(2)}) copy-start(f32[512,256]{1,0:T(8,128)} %get-tuple-element.14) | copy-start | bytes 1572868

commit v5 on v4

--- a/solution.py
+++ b/solution.py
@@ -429,9 +429,9 @@
 
 def gathered_kernel(
     st_n, tp_n, depth, pass_len,
-    ids_ref, store_ref, q_hbm, g_hbm, wq_hbm, wg_hbm, wk_hbm, wv_hbm, m_hbm,
-    tok_out, store_out, wkey_out,
-    rows, wall, wqg, q_v, g_v, m_v, acc, terms, k_all, v_all, ask_v, ask_in, order_v, req_ref, gated, slope, ret, prob_v, kvb, reqg, gboth, arr,
+    ids_hbm, store_ref, q_hbm, g_hbm, wq_hbm, wg_hbm, wk_hbm, wv_hbm, m_hbm,
+    tok_hbm, store_hbm, wkey_hbm,
+    ids_ref, tok_out, store_out, wkey_out, rows, wall, wqg, q_v, g_v, m_v, acc, terms, k_all, v_all, ask_v, ask_in, order_v, req_ref, gated, slope, ret, prob_v, kvb, reqg, gboth, arr,
     hot, plow, sums, dwp, dwc, dwf, tp_part, tp_pair, tp_recv,
     lsem, gs, gr, fs, fr, zs, zr, ps, pr, xs, xr, ws, wr, ss, sr, us, ur,
 ):
@@ -461,6 +461,7 @@
         copy.start()
         return copy
 
+    ids_copy = local(9, ids_hbm, ids_ref)
     own_rows = local(0, store_ref, rows.at[tp])
     loads_kv = [
         local(1, wk_hbm, wall.at[tp, :, pl.ds(0, cols)]),
@@ -488,6 +489,8 @@
             barrier, inc=1, device_id={"tp": (tp + d) % tp_n}, device_id_type=MESH
         )
     pl.semaphore_signal(barrier, inc=1, device_id=twin, device_id_type=MESH)
+
+    ids_copy.wait()
 
     def plan(wide):
         line = lax.broadcasted_iota(jnp.int32, (8, wide), 0)
@@ -572,31 +575,34 @@
     ask_in[st] = ask_v[st]
     order_copy = local(8, order_v, req_ref)
 
-    def project(i, send):
-        r = pl.ds(first_row(i), some_rows)
+    def project(i, count, send):
+        r = pl.ds(first_row(i), count * some_rows)
 
         def term(t, span):
             return dot(rows[t, r], wall[tp, pl.ds(pl.multiple_of(t * chunk, chunk), chunk), span])
 
-        for d in range(1, hi_n):
-            g_wait(((hi + d) % hi_n) * 2 + lo, i)
-            onward(d, i).start()
-        g_wait(mate_t, i)
+        for q in range(count):
+            for d in range(1, hi_n):
+                g_wait(((hi + d) % hi_n) * 2 + lo, i + q)
+                onward(d, i + q).start()
+            g_wait(mate_t, i + q)
         near = [tp, mate_t] + [((hi + d) % hi_n) * 2 + lo for d in range(1, hi_n)]
         late = [((hi + d) % hi_n) * 2 + 1 - lo for d in range(1, hi_n)]
         total = sum(term(t, key_cols) for t in near[1:]) + term(near[0], key_cols)
         for t in late:
-            g_wait(t, i)
+            for q in range(count):
+                g_wait(t, i + q)
             total = total + term(t, key_cols)
-        low = total.astype(BF)
         first = st * passages + first_row(i) // pass_len
-        for p in range(some):
-            k_all[first + p] = low[p * pass_len : (p + 1) * pass_len]
+
+        def keep(ref, total):
+            low = total.astype(BF)
+            for p in range(count * some):
+                ref[first + p] = low[p * pass_len : (p + 1) * pass_len]
+
+        keep(k_all, total)
         send()
-        total = sum(term(t, value_cols) for t in near + late)
-        low = total.astype(BF)
-        for p in range(some):
-            v_all[first + p] = low[p * pass_len : (p + 1) * pass_len]
+        keep(v_all, sum(term(t, value_cols) for t in near + late))
 
     def part_of_all(kind, o, c, side):
         ref = k_all if kind == 0 else v_all
@@ -675,9 +681,9 @@
         slope[r, :] = grad * (sig * (1.0 + gate * (1.0 - sig)))
 
     def early_step(i, c):
-        project(i, lambda: own_send(0, i))
-
-        @pl.when(i > 0)
+        project(i, 1, lambda: own_send(0, i))
+
+        @pl.when(i >= 1)
         def _():
             relay(0, 1, i - 1)
 
@@ -689,7 +695,8 @@
         return c
 
     lax.fori_loop(0, n_some, early_step, 0)
-    relay(0, 1, n_some - 1)
+    for i in range(n_some - 1, n_some):
+        relay(0, 1, i)
 
     def inward_send(i, c):
         own_send(1, i, outward=False)
@@ -708,16 +715,18 @@
     lax.fori_loop(0, n_some, second_step, 0)
     lax.fori_loop(0, n_some, outward_send, 0)
 
+    n_part = tile_of(n_some, 2)
+
     def late_step(i, c):
-        project(n_some + i, lambda: None)
-
-        @pl.when(edge)
-        def _():
-            relay(0, 3, i)
-
-        @pl.when(jnp.logical_not(edge))
-        def _():
-            relay(1, 1, i)
+        project(n_some + i * n_part, n_part, lambda: None)
+        for q in range(n_part):
+            @pl.when(edge)
+            def _():
+                relay(0, 3, i * n_part + q)
+
+            @pl.when(jnp.logical_not(edge))
+            def _():
+                relay(1, 1, i * n_part + q)
 
         return c
 
@@ -756,7 +765,7 @@
         lax.fori_loop(first, last, step, 0)
 
     relays = (st_n - 1) * n_some
-    lax.fori_loop(0, n_some, late_step, 0)
+    lax.fori_loop(0, n_some // n_part, late_step, 0)
     w_beside.start()
     relay_rest(1, 0, jnp.where(edge, n_some, 0))
     for copy in loads_q[3:]:
@@ -769,19 +778,21 @@
         for j in range(PB):
             kvb[n, j * pass_len : (j + 1) * pass_len, span] = ref[ids_ref[j, b]]
 
-    pairs = range(2)
+    pairs = range(4)
 
     def block_rows(b):
         return pl.ds(pl.multiple_of(b * BLK, BLK), BLK)
 
+    per_step = n_some // (blocks // 4)
+
     def probs_step(i, c):
         for n in pairs:
-            fill(n, k_all, key_cols, 2 * i + n)
+            fill(n, k_all, key_cols, 4 * i + n)
         for head in range(heads):
             hs = slice(head * HD, (head + 1) * HD)
             vs = slice(cols + head * HD, cols + (head + 1) * HD)
             for n in pairs:
-                b = 2 * i + n
+                b = 4 * i + n
                 r = block_rows(b)
                 scores = dot(q_v[r, hs], kvb[n, :, hs], NT) * scale
                 shifted = jnp.exp(scores - jnp.max(scores, axis=-1, keepdims=True))
@@ -791,13 +802,12 @@
                 for j in range(PB):
                     reqg[j * blocks + b, :, vs] = value_grad[j * pass_len : (j + 1) * pass_len]
 
-        @pl.when(i < n_some)
-        def _():
-            relay(1, 2, i)
-
-        return c
-
-    lax.fori_loop(0, blocks // 2, probs_step, 0)
+        for q in range(per_step):
+            relay(1, 2, i * per_step + q)
+
+        return c
+
+    lax.fori_loop(0, blocks // 4, probs_step, 0)
 
     def half(ref, peer, part):
         return ref.at[peer, :, :, part]
@@ -830,18 +840,18 @@
         1, vs_all, value_cols, value_peer, 1, jnp.where(edge, st_n, st_n - 1)
     )
     keep_own(value_cols)
-    relay_rest(1, n_some + min(n_some, blocks // 2), relays)
+    relay_rest(1, n_some + per_step * (blocks // 4), relays)
     twin_wait(1)
 
     def block_step(i, c):
         for n in pairs:
-            fill(n, k_all, key_cols, 2 * i + n)
-            fill(n, v_all, value_cols, 2 * i + n)
+            fill(n, k_all, key_cols, 4 * i + n)
+            fill(n, v_all, value_cols, 4 * i + n)
         for head in range(heads):
             hs = slice(head * HD, (head + 1) * HD)
             vs = slice(cols + head * HD, cols + (head + 1) * HD)
             for n in pairs:
-                b = 2 * i + n
+                b = 4 * i + n
                 r = block_rows(b)
                 value = kvb[n, :, vs]
                 prob = prob_v[head, r, :]
@@ -856,8 +866,11 @@
                 gboth[r, vs] = (attended * slope[r, hs]).astype(BF)
         return c
 
-    lax.fori_loop(0, blocks // 2, block_step, 0)
-    give_back(2, ks, key_cols, far_peer, 1, st_n)
+    lax.fori_loop(0, blocks // 4, block_step, 0)
+    def key_peer(d):
+        return jnp.where(edge, near_peer(jnp.where(d == 1, 1, st_n + 1 - d)), far_peer(d))
+
+    give_back(2, ks, key_cols, key_peer, 1, st_n)
     keep_own(key_cols)
 
     n_tile = tile_of(model, 512)
@@ -1074,6 +1087,7 @@
     for d in range(1, hi_n):
         total = total + tp_recv[(hi + d) % hi_n].astype(F32)
     tok_out[...] = total.astype(BF)
+    tok_done = local(10, tok_out, tok_hbm)
 
     @pl.when(inner)
     def _():
@@ -1082,6 +1096,7 @@
     for d in range(1, tp_n):
         sums_wait(1, vs_all, (tp + d) % tp_n)
     store_terms(value_cols, keep_store)
+    store_done = local(11, store_out, store_hbm)
 
     for b in range(bits):
         line = slice(b * bit, (b + 1) * bit)
@@ -1095,6 +1110,8 @@
                 dw_copy(kind, b).wait_recv()
 
         wkey_out[line, :] += dwf[1, line, :].astype(F32)
+
+    wkey_done = local(12, wkey_out, wkey_hbm)
 
     def wait_send(copy):
         copy.wait_send()
@@ -1149,6 +1166,45 @@
             @pl.when(inner)
             def _():
                 dw_copy(3 + q, b).wait_send()
+    for copy in (tok_done, store_done, wkey_done):
+        copy.wait()
+
+
+def settle_kernel(*refs):
+    n = (len(refs) - 2) // 3
+    sources, results, held = refs[:n], refs[n : 2 * n], refs[2 * n : 3 * n]
+    ins, outs = refs[3 * n], refs[3 * n + 1]
+    pieces = []
+    for a, (source, result, here) in enumerate(zip(sources, results, held)):
+        part = source.shape[0] // 2
+        for i in range(2):
+            r = pl.ds(i * part, part)
+            pieces.append(
+                (
+                    pltpu.make_async_copy(source.at[r], here.at[r], ins.at[a, i]),
+                    pltpu.make_async_copy(here.at[r], result.at[r], outs.at[a, i]),
+                )
+            )
+    for fetch, _ in pieces:
+        fetch.start()
+    for fetch, put in pieces:
+        fetch.wait()
+        put.start()
+    for _, put in pieces:
+        put.wait()
+
+
+def settle(*arrays):
+    hbm = pl.BlockSpec(memory_space=pl.ANY)
+    n = len(arrays)
+    return pl.pallas_call(
+        settle_kernel,
+        out_shape=tuple(jax.ShapeDtypeStruct(a.shape, a.dtype) for a in arrays),
+        in_specs=[hbm] * n,
+        out_specs=(hbm,) * n,
+        scratch_shapes=[pltpu.VMEM(a.shape, a.dtype) for a in arrays]
+        + [pltpu.SemaphoreType.DMA((n, 2)), pltpu.SemaphoreType.DMA((n, 2))],
+    )(*arrays)
 
 
 def local(pass_ids, store, queries, gate_pre, w_query, w_gate, w_key, w_value, d_mem):
@@ -1175,7 +1231,10 @@
     hot_cols = depth * pass_len
     width = -(-hot_cols // 128) * 128
     gathered_bytes = 2 * 2 * st_n * pass_rows * cols
-    if lax.axis_size("grp") == 2 and hi_n == 2 and st_n == 4 and passages % 2 == 0 and gathered_bytes <= 8 << 20:
+    steps = blocks // 4
+    fits = lax.axis_size("grp") == 2 and hi_n == 2 and st_n == 4 and st_n == tp_n
+    fits = fits and passages % 4 == 0 and blocks % 4 == 0 and passages // 4 % steps == 0
+    if fits and gathered_bytes <= 8 << 20:
         half_pass = passages // 2
         n_some = half_pass // tile_of(half_pass, 2)
         d_tokens, d_store, d_wkey = pl.pallas_call(
@@ -1185,9 +1244,13 @@
                 jax.ShapeDtypeStruct((sto_pair, model), BF),
                 jax.ShapeDtypeStruct((share, cols), F32),
             ),
-            in_specs=[smem] + [hbm] * 8,
-            out_specs=(vmem, vmem, vmem),
+            in_specs=[hbm] * 9,
+            out_specs=(hbm, hbm, hbm),
             scratch_shapes=[
+                pltpu.SMEM((PB, blocks), jnp.int32),
+                V((tok_pair, model), BF),
+                V((sto_pair, model), BF),
+                V((share, cols), F32),
                 V((tp_n, pass_rows, chunk), BF),
                 V((tp_n, model, pair), BF),
                 V((model, pair), BF),
@@ -1206,7 +1269,7 @@
                 V((tok_rows, cols), F32),
                 V((st_n, depth, pass_len, pair), BF),
                 V((cols // HD, tok_rows, PB * pass_len), F32),
-                V((2, PB * pass_len, pair), BF),
+                V((4, PB * pass_len, pair), BF),
                 V((requests, pass_len, pair), BF),
                 V((tok_rows, pair), BF),
                 V((st_n, depth, pass_len, pair), BF),
@@ -1219,7 +1282,7 @@
                 V((tp_n, tok_pair, model), BF),
                 V((hi_n, tok_pair, model), BF),
                 V((hi_n, tok_pair, model), BF),
-                DMA((9,)),
+                DMA((13,)),
                 DMA((3, hi_n, 2 * n_some)),
                 DMA((tp_n, 2 * n_some)),
                 DMA((2, st_n, n_some, 3)),
@@ -1244,6 +1307,7 @@
             pass_ids.T, store.reshape(pass_rows, chunk),
             queries, gate_pre, w_query, w_gate, w_key, w_value, d_mem,
         )
+        d_tokens, d_store, d_wkey = settle(d_tokens, d_store, d_wkey)
         return d_tokens, d_store.reshape(passages // tp_n, pass_len, model), d_wkey
 
     ids = pass_ids.reshape(-1)

time: 112 us -> 108 us (0.964)
  local copies, waits for them, and re-layouts: 4.59 us -> 0 us
    unnamed x7 -> x0, local copies, waits for them, and re-layouts: 4.59 us -> none
    pallas_call x1, Pallas kernels: 107 us -> 104 us  [local(): pl.pallas_call(functools.partial(gathered_kernel, st_n, tp_n, depth, pass...]
    pallas_call x0 -> x1, Pallas kernels: none -> 2.63 us  [settle(): pl.pallas_call(settle_kernel, out_shape=tuple((jax.ShapeDtypeStruct(a.sha...]
where the time goes in v5:
time: 108 us; the launch traced here: 107 us
  Pallas kernels  107 us (99%)
    pallas_call x1, Pallas kernels, local(): pl.pallas_call(functools.partial(gathered_kernel, st_n, tp_n, depth, pass...  104 us
    pallas_call x1, Pallas kernels, settle(): pl.pallas_call(settle_kernel, out_shape=tuple((jax.ShapeDtypeStruct(a.sha...  2.63 us

profile of v5, /device:TPU:1, one launch (start us, length us, event | category | flops | bytes accessed | tf_op | source)
XLA Modules:
  0.0 107.5 jit_solution(4103698712969626516)
XLA Ops:
  0.6 104.2 %shard_map.112 = (bf16[256,2048]{1,0:T(8,128)(2,1)}, bf16[256,2048]{1,0:T(8,128)(2,1)}, f32[512,256]{1,0:T(8,128)}) custom-call(s32[4,8]{1,0:T(4,128)} %bitcast.4, bf16[1024,512]{1,0:T(8,128)(2,1)} %bitcast.3, bf16[1024,256]{1,0:T(8,128)(2,1)} %q_hbm.1, bf16[1024,256]{1,0:T(8,128)(2,1)} %g_hbm.1, bf16[2048,256]{1,0:T(8,128)(2,1)} %wq_hbm.1, ...), custom_call_target="tpu_custom_call" | custom-call | tf_op jit(solution)/shard_map/pallas_call | solution.py:1240
  104.8 2.6 %shard_map.113 = (bf16[256,2048]{1,0:T(8,128)(2,1)}, bf16[256,2048]{1,0:T(8,128)(2,1)}, f32[512,256]{1,0:T(8,128)}) custom-call(bf16[256,2048]{1,0:T(8,128)(2,1)} %get-tuple-element.9.refs_0_, bf16[256,2048]{1,0:T(8,128)(2,1)} %get-tuple-element.10.refs_1_, f32[512,256]{1,0:T(8,128)} %get-tuple-element.11.refs_2_), custom_call_target="tpu_custom_call" | custom-call | tf_op jit(solution)/shard_map/pallas_call | solution.py:1200

commit v6 on v5

--- a/solution.py
+++ b/solution.py
@@ -433,7 +433,7 @@
     tok_hbm, store_hbm, wkey_hbm,
     ids_ref, tok_out, store_out, wkey_out, rows, wall, wqg, q_v, g_v, m_v, acc, terms, k_all, v_all, ask_v, ask_in, order_v, req_ref, gated, slope, ret, prob_v, kvb, reqg, gboth, arr,
     hot, plow, sums, dwp, dwc, dwf, tp_part, tp_pair, tp_recv,
-    lsem, gs, gr, fs, fr, zs, zr, ps, pr, xs, xr, ws, wr, ss, sr, us, ur,
+    lsem, gs, gr, fs, fr, fw, zs, zr, ps, pr, xs, xr, ws, wr, ss, sr, us, ur,
 ):
     grp = lax.axis_index("grp")
     st = lax.axis_index("st")
@@ -461,19 +461,19 @@
         copy.start()
         return copy
 
-    ids_copy = local(9, ids_hbm, ids_ref)
+    def sent(ref, sem):
+        remote(ref, ref, sem, pr.at[0], mate).wait_send()
+
+    def landed(ref, sem):
+        remote(ref, ref, ps.at[0], sem, mate).wait_recv()
+
+    ids_copy = local(7, ids_hbm, ids_ref)
     own_rows = local(0, store_ref, rows.at[tp])
-    loads_kv = [
-        local(1, wk_hbm, wall.at[tp, :, pl.ds(0, cols)]),
-        local(2, wv_hbm, wall.at[tp, :, pl.ds(cols, cols)]),
-    ]
-    loads_q = [
-        local(3, q_hbm, q_v),
-        local(4, g_hbm, g_v),
-        local(5, m_hbm, m_v),
-        local(6, wq_hbm, wqg.at[:, pl.ds(0, cols)]),
-        local(7, wg_hbm, wqg.at[:, pl.ds(cols, cols)]),
-    ]
+    local(1, wk_hbm, wall.at[tp, :, pl.ds(0, cols)])
+    local(1, wv_hbm, wall.at[tp, :, pl.ds(cols, cols)])
+    loads_q = [local(2, q_hbm, q_v), local(3, g_hbm, g_v), local(4, m_hbm, m_v)]
+    local(5, wq_hbm, wqg.at[:, pl.ds(0, cols)])
+    local(5, wg_hbm, wqg.at[:, pl.ds(cols, cols)])
 
     barrier = pltpu.get_barrier_semaphore()
 
@@ -525,32 +525,42 @@
         part = (grp + i // n_some) % 2
         return pl.multiple_of((part * n_some + i % n_some) * some_rows, some_rows)
 
-    def g_copy(way, i, t, source, peer, slot):
-        r = pl.ds(first_row(i), some_rows)
-        return remote(rows.at[source, r], rows.at[t, r], gs.at[way, slot, i], gr.at[t, i], peer)
-
-    def across(d, i):
-        h = (hi + d) % hi_n
-        return g_copy(0, i, tp, tp, {"tp": h * 2 + lo}, h)
-
-    def beside(i):
-        return g_copy(1, i, tp, tp, mate, hi)
-
-    def onward(d, i):
-        h = (hi + d) % hi_n
-        return g_copy(2, i, h * 2 + lo, h * 2 + lo, mate, h)
-
-    def g_wait(t, i):
-        g_copy(1, i, t, t, mate, hi).wait_recv()
-
-    def rows_send(i, c):
+    n_part = tile_of(n_some, 2)
+
+    def g_copy(way, lot, t, onto):
+        i, count, slot = lot
+        r = pl.ds(first_row(i), count * some_rows)
+        away = (t - onto + tp_n) % tp_n - 1
+        return remote(rows.at[t, r], rows.at[t, r], gs.at[way], gr.at[away, slot], {"tp": onto})
+
+    def small(i):
+        return i, 1, i
+
+    def large(i):
+        return n_some + i * n_part, n_part, n_some + i
+
+    def onward(d, lot):
+        return g_copy(2, lot, ((hi + d) % hi_n) * 2 + lo, mate_t)
+
+    def g_wait(t, lot):
+        g_copy(1, lot, t, tp).wait_recv()
+
+    def rows_send(lot):
         for d in range(1, hi_n):
-            across(d, i).start()
-        beside(i).start()
+            g_copy(0, lot, tp, ((hi + d) % hi_n) * 2 + lo).start()
+        g_copy(1, lot, tp, mate_t).start()
+
+    def rows_small(i, c):
+        rows_send(small(i))
+        return c
+
+    def rows_large(i, c):
+        rows_send(large(i))
         return c
 
     own_rows.wait()
-    lax.fori_loop(0, 2 * n_some, rows_send, 0)
+    lax.fori_loop(0, n_some, rows_small, 0)
+    lax.fori_loop(0, n_some // n_part, rows_large, 0)
 
     upper = st >= st_n // 2
     mark = jnp.where(upper, st, st_n - 1 - st)
@@ -561,10 +571,11 @@
         return jnp.where(upper, i, st_n - 1 - i)
 
     def z_copy(phase, src, dst, peer):
-        return remote(src, dst, zs.at[phase, peer], zr.at[phase, st], {"st": peer})
+        away = (st - peer + st_n) % st_n - 1
+        return remote(src, dst, zs.at[phase], zr.at[phase, away], {"st": peer})
 
     def z_wait(phase, src, dst, peer):
-        remote(src, dst, zs.at[phase, peer], zr.at[phase, peer], {"st": peer}).wait_recv()
+        landed(dst, zr.at[phase, (peer - st + st_n) % st_n - 1])
 
     def ask_send(d, c):
         peer = (st + d) % st_n
@@ -573,25 +584,24 @@
 
     lax.fori_loop(1, st_n, ask_send, 0)
     ask_in[st] = ask_v[st]
-    order_copy = local(8, order_v, req_ref)
-
-    def project(i, count, send):
+    order_copy = local(6, order_v, req_ref)
+
+    def project(lot, send):
+        i, count, _ = lot
         r = pl.ds(first_row(i), count * some_rows)
 
         def term(t, span):
             return dot(rows[t, r], wall[tp, pl.ds(pl.multiple_of(t * chunk, chunk), chunk), span])
 
-        for q in range(count):
-            for d in range(1, hi_n):
-                g_wait(((hi + d) % hi_n) * 2 + lo, i + q)
-                onward(d, i + q).start()
-            g_wait(mate_t, i + q)
+        for d in range(1, hi_n):
+            g_wait(((hi + d) % hi_n) * 2 + lo, lot)
+            onward(d, lot).start()
+        g_wait(mate_t, lot)
         near = [tp, mate_t] + [((hi + d) % hi_n) * 2 + lo for d in range(1, hi_n)]
         late = [((hi + d) % hi_n) * 2 + 1 - lo for d in range(1, hi_n)]
         total = sum(term(t, key_cols) for t in near[1:]) + term(near[0], key_cols)
         for t in late:
-            for q in range(count):
-                g_wait(t, i + q)
+            g_wait(t, lot)
             total = total + term(t, key_cols)
         first = st * passages + first_row(i) // pass_len
 
@@ -608,20 +618,20 @@
         ref = k_all if kind == 0 else v_all
         return ref.at[pl.ds(o * passages + side * half_pass + c * some, some)]
 
-    def chain_copy(kind, o, c, way, peer):
+    def chain_copy(kind, o, c, peer):
         part = part_of_all(kind, o, c, grp)
-        return remote(part, part, fs.at[kind, o, c, way], fr.at[kind, o, c, 0], {"st": peer})
+        away = (o - peer + st_n) % st_n - 1
+        return remote(part, part, fs.at[kind, 0], fr.at[kind, away, c], {"st": peer})
 
     def twin_copy(kind, o, c):
         part = part_of_all(kind, o, c, grp)
-        return remote(part, part, fs.at[kind, o, c, 2], fr.at[kind, o, c, 1], twin)
+        return remote(part, part, fs.at[kind, 1], fw.at[kind], twin)
 
     lower = st < st_n // 2
     edge = (st == 0) | (st == st_n - 1)
 
-    def own_copies(kind, c, act, inward=True, outward=True):
-        ways = ((0, st + 1, lower), (1, st - 1, jnp.logical_not(lower)))
-        for way, onto, toward in ways:
+    def own_send(kind, c, inward=True, outward=True):
+        for onto, toward in ((st + 1, lower), (st - 1, jnp.logical_not(lower))):
             there = (onto >= 0) & (onto < st_n)
             if not outward:
                 there = there & toward
@@ -630,44 +640,30 @@
 
             @pl.when(there)
             def _():
-                act(chain_copy(kind, st, c, way, onto))
-
-    def relay_copies(kind, d, c, act, ready):
-        for way, sign in ((0, -1), (1, 1)):
+                chain_copy(kind, st, c, onto).start()
+
+    def relay(kind, d, c):
+        for sign in (-1, 1):
             o = st + sign * d
             onto = st - sign
 
             @pl.when((o >= 0) & (o < st_n))
             def _():
-                if ready:
-                    chain_copy(kind, o, c, way, st).wait_recv()
+                chain_copy(kind, o, c, st).wait_recv()
 
                 @pl.when((onto >= 0) & (onto < st_n))
                 def _():
-                    act(chain_copy(kind, o, c, way, onto))
-
-                act(twin_copy(kind, o, c))
-
-    def start(copy):
-        copy.start()
-
-    def own_send(kind, c, **which):
-        own_copies(kind, c, start, **which)
-
-    def relay(kind, d, c):
-        relay_copies(kind, d, c, start, True)
+                    chain_copy(kind, o, c, onto).start()
+
+                twin_copy(kind, o, c).start()
+
+    relayed = (st_n - 1) * half_pass
 
     def twin_wait(kind):
-        def step(i, c):
-            o = (st + 1 + i // n_some) % st_n
-            k = i % n_some
-            part = part_of_all(kind, o, k, 1 - grp)
-            remote(part, part, fs.at[kind, o, k, 2], fr.at[kind, o, k, 1], twin).wait_recv()
-            return c
-
-        lax.fori_loop(0, (st_n - 1) * n_some, step, 0)
-
-    for copy in loads_kv + loads_q[:3]:
+        landed((k_all, v_all)[kind].at[pl.ds(0, relayed)], fw.at[kind])
+
+    landed(wall.at[tp], lsem.at[1])
+    for copy in loads_q:
         copy.wait()
 
     gate_rows = tok_rows // n_some
@@ -681,7 +677,7 @@
         slope[r, :] = grad * (sig * (1.0 + gate * (1.0 - sig)))
 
     def early_step(i, c):
-        project(i, 1, lambda: own_send(0, i))
+        project(small(i), lambda: own_send(0, i))
 
         @pl.when(i >= 1)
         def _():
@@ -715,10 +711,8 @@
     lax.fori_loop(0, n_some, second_step, 0)
     lax.fori_loop(0, n_some, outward_send, 0)
 
-    n_part = tile_of(n_some, 2)
-
     def late_step(i, c):
-        project(n_some + i * n_part, n_part, lambda: None)
+        project(large(i), lambda: None)
         for q in range(n_part):
             @pl.when(edge)
             def _():
@@ -737,22 +731,22 @@
     def w_across(d):
         h = (hi + d) % hi_n
         part = wall.at[tp, w_mine]
-        return remote(part, part, ws.at[0, h], wr.at[0, tp], {"tp": h * 2 + lo})
+        return remote(part, part, ws.at[0], wr.at[0], {"tp": h * 2 + lo})
 
     def w_twin(d):
         t = ((hi + d) % hi_n) * 2 + lo
         part = wall.at[t, w_mine]
-        return remote(part, part, ws.at[1, (hi + d) % hi_n], wr.at[1, t], twin)
+        return remote(part, part, ws.at[0], wr.at[1], twin)
 
     def w_onward(d, k):
         t = ((hi + d) % hi_n) * 2 + lo
         part = wall.at[t, w_other if k else w_mine]
-        return remote(part, part, ws.at[2 + k, (hi + d) % hi_n], wr.at[2 + k, t], mate)
-
-    w_beside = remote(wall.at[tp], wall.at[tp], ws.at[4, 0], wr.at[4, tp], mate)
+        return remote(part, part, ws.at[0], wr.at[2], mate)
+
+    w_beside = remote(wall.at[tp], wall.at[tp], ws.at[0], wr.at[2], mate)
 
     def w_wait(kind, t, part):
-        remote(wall.at[t, part], wall.at[t, part], ws.at[kind, 0], wr.at[kind, t], mate).wait_recv()
+        landed(wall.at[t, part], wr.at[kind])
 
     for d in range(1, hi_n):
         w_across(d).start()
@@ -768,8 +762,7 @@
     lax.fori_loop(0, n_some // n_part, late_step, 0)
     w_beside.start()
     relay_rest(1, 0, jnp.where(edge, n_some, 0))
-    for copy in loads_q[3:]:
-        copy.wait()
+    landed(wqg, lsem.at[5])
     order_copy.wait()
     twin_wait(0)
     scale = HD ** (-0.5)
@@ -888,11 +881,11 @@
         lax.fori_loop(0, model // n_tile, step, 0)
 
     def pair_copy(h):
-        return remote(tp_part.at[h * 2 + 1 - lo], tp_pair.at[h], ps.at[h], pr.at[h], mate)
+        return remote(tp_part.at[h * 2 + 1 - lo], tp_pair.at[h], ps.at[0], pr.at[h], mate)
 
     def cross(h):
         return remote(
-            tp_part.at[h * 2 + lo], tp_recv.at[hi], xs.at[h], xr.at[hi], {"tp": h * 2 + lo}
+            tp_part.at[h * 2 + lo], tp_recv.at[hi], xs.at[0], xr.at[0], {"tp": h * 2 + lo}
         )
 
     for d in range(1, hi_n):
@@ -943,11 +936,10 @@
     def sums_copy(kind, part, d):
         t = (tp + d) % tp_n
         src = plow.at[pl.ds(pl.multiple_of(t * sto_pair, sto_pair), sto_pair), part]
-        return remote(src, sums.at[tp, :, part], ss.at[kind, t], sr.at[kind, tp], {"tp": t})
-
-    def sums_wait(kind, part, t):
-        dst = sums.at[t, :, part]
-        remote(dst, dst, ss.at[kind, t], sr.at[kind, t], mate).wait_recv()
+        return remote(src, sums.at[tp, :, part], ss.at[kind], sr.at[kind], {"tp": t})
+
+    def sums_of(part):
+        return sums.at[pl.ds(0, tp_n - 1), :, part]
 
     def grads_of(kind, peer):
         phase, part, span = (2, ks, key_cols) if kind == 0 else (1, vs_all, value_cols)
@@ -998,7 +990,7 @@
         else:
             src, dst = dwc.at[kind - 3, line], dwf.at[1, line]
             peer = middle if kind == 4 else beyond
-        return remote(src, dst, us.at[kind, b], ur.at[kind, b], {"st": peer})
+        return remote(src, dst, us.at[0], ur.at[min(kind, 3), b], {"st": peer})
 
     def dw_send(kind):
         for b in range(bits):
@@ -1047,11 +1039,7 @@
         t = ((hi + d) % hi_n) * 2 + lo
         w_wait(1, t, w_other)
         w_onward(d, 1).start()
-    w_wait(4, mate_t, pl.ds(0, model))
-    for d in range(1, hi_n):
-        t = ((hi + d) % hi_n) * 2 + 1 - lo
-        w_wait(2, t, w_mine)
-        w_wait(3, t, w_other)
+    landed(wall.at[pl.ds(0, hi_n)], wr.at[2])
 
     def store_terms(span, done):
         def step(i, c):
@@ -1073,30 +1061,26 @@
     grads_of(1, jnp.where(outer, middle, beyond))
     sums_send(1)
 
-    for d in range(1, tp_n):
-        sums_wait(0, ks, (tp + d) % tp_n)
+    landed(sums_of(ks), sr.at[0])
     store_terms(key_cols, keep_terms)
 
     pair_copy(hi).wait_recv()
     for d in range(1, hi_n):
         h = (hi + d) % hi_n
-        remote(
-            tp_part.at[h * 2 + lo], tp_recv.at[h], xs.at[h], xr.at[h], {"tp": h * 2 + lo}
-        ).wait_recv()
+        landed(tp_recv.at[h], xr.at[0])
     total = tp_part[tp].astype(F32) + tp_pair[hi].astype(F32)
     for d in range(1, hi_n):
         total = total + tp_recv[(hi + d) % hi_n].astype(F32)
     tok_out[...] = total.astype(BF)
-    tok_done = local(10, tok_out, tok_hbm)
+    tok_done = local(2, tok_out, tok_hbm)
 
     @pl.when(inner)
     def _():
         dw_relay(1)
 
-    for d in range(1, tp_n):
-        sums_wait(1, vs_all, (tp + d) % tp_n)
+    landed(sums_of(vs_all), sr.at[1])
     store_terms(value_cols, keep_store)
-    store_done = local(11, store_out, store_hbm)
+    store_done = local(3, store_out, store_hbm)
 
     for b in range(bits):
         line = slice(b * bit, (b + 1) * bit)
@@ -1111,61 +1095,28 @@
 
         wkey_out[line, :] += dwf[1, line, :].astype(F32)
 
-    wkey_done = local(12, wkey_out, wkey_hbm)
-
-    def wait_send(copy):
-        copy.wait_send()
-
-    def rows_drain(i, c):
-        for d in range(1, hi_n):
-            across(d, i).wait_send()
-            onward(d, i).wait_send()
-        beside(i).wait_send()
-        return c
-
-    lax.fori_loop(0, 2 * n_some, rows_drain, 0)
-
-    def all_drain(i, c):
-        for kind in (0, 1):
-            own_copies(kind, i, wait_send)
-            for d in range(1, st_n):
-                relay_copies(kind, d, i, wait_send, False)
-        return c
-
-    lax.fori_loop(0, n_some, all_drain, 0)
-    for d in range(1, hi_n):
-        w_across(d).wait_send()
-        w_twin(d).wait_send()
-        w_onward(d, 0).wait_send()
-        w_onward(d, 1).wait_send()
-    w_beside.wait_send()
-
-    def drain(d, c):
-        peer = (st + d) % st_n
-        z_copy(0, ask_v.at[peer], ask_in.at[st], peer).wait_send()
-        back_copy(1, vs_all, peer).wait_send()
-        back_copy(2, ks, peer).wait_send()
-        return c
-
-    lax.fori_loop(1, st_n, drain, 0)
-    for d in range(1, tp_n):
-        sums_copy(0, ks, d).wait_send()
-        sums_copy(1, vs_all, d).wait_send()
-    for d in range(1, hi_n + 1):
-        h = (hi + d) % hi_n
-        pair_copy(h).wait_send()
-        if d < hi_n:
-            cross(h).wait_send()
-    for b in range(bits):
-        dw_copy(2, b).wait_send()
-        for q in (0, 1):
-            @pl.when(outer)
+    wkey_done = local(4, wkey_out, wkey_hbm)
+
+    for way in range(3):
+        sent(rows.at[tp], gs.at[way])
+    for kind, ref in ((0, k_all), (1, v_all)):
+        sent(ref.at[pl.ds(0, relayed)], fs.at[kind, 1])
+        for s in range(st_n):
+            up, down = (s + 1) * (s + 1 < st_n), (st_n - s) * (s > 0)
+
+            @pl.when(st == s)
             def _():
-                dw_copy(q, b).wait_send()
-
-            @pl.when(inner)
-            def _():
-                dw_copy(3 + q, b).wait_send()
+                sent(ref.at[pl.ds(0, (up + down) * half_pass)], fs.at[kind, 0])
+
+    sent(wall.at[pl.ds(0, hi_n + 1)], ws.at[0])
+    sent(ask_in.at[pl.ds(0, st_n - 1)], zs.at[0])
+    sent(ret.at[pl.ds(0, st_n - 1), :, :, vs_all], zs.at[1])
+    sent(ret.at[pl.ds(0, st_n - 1), :, :, ks], zs.at[2])
+    sent(sums_of(ks), ss.at[0])
+    sent(sums_of(vs_all), ss.at[1])
+    sent(tp_pair, ps.at[0])
+    sent(tp_recv.at[0], xs.at[0])
+    sent(dwp.at[pl.ds(0, 3 * share)], us.at[0])
     for copy in (tok_done, store_done, wkey_done):
         copy.wait()
 
@@ -1282,23 +1233,24 @@
                 V((tp_n, tok_pair, model), BF),
                 V((hi_n, tok_pair, model), BF),
                 V((hi_n, tok_pair, model), BF),
-                DMA((13,)),
-                DMA((3, hi_n, 2 * n_some)),
-                DMA((tp_n, 2 * n_some)),
-                DMA((2, st_n, n_some, 3)),
-                DMA((2, st_n, n_some, 2)),
-                DMA((3, st_n)),
-                DMA((3, st_n)),
+                DMA((8,)),
+                DMA((3,)),
+                DMA((tp_n - 1, n_some + n_some // tile_of(n_some, 2))),
+                DMA((2, 2)),
+                DMA((2, st_n - 1, n_some)),
+                DMA((2,)),
+                DMA((3,)),
+                DMA((3, st_n - 1)),
+                DMA((1,)),
                 DMA((hi_n,)),
-                DMA((hi_n,)),
-                DMA((hi_n,)),
-                DMA((hi_n,)),
-                DMA((5, hi_n)),
-                DMA((5, tp_n)),
-                DMA((2, tp_n)),
-                DMA((2, tp_n)),
-                DMA((5, 2)),
-                DMA((5, 2)),
+                DMA((1,)),
+                DMA((1,)),
+                DMA((1,)),
+                DMA((3,)),
+                DMA((2,)),
+                DMA((2,)),
+                DMA((1,)),
+                DMA((4, 2)),
             ],
             compiler_params=pltpu.CompilerParams(
                 collective_id=0, has_side_effects=True, vmem_limit_bytes=67043328

time: 108 us -> 105 us (0.972)
  Pallas kernels: 107 us -> 104 us
    pallas_call x1, Pallas kernels: 104 us -> 102 us  [local(): pl.pallas_call(functools.partial(gathered_kernel, st_n, tp_n, depth, pass...]
where the time goes in v6:
time: 105 us
  Pallas kernels  104 us (99%)
    pallas_call x1, Pallas kernels, local(): pl.pallas_call(functools.partial(gathered_kernel, st_n, tp_n, depth, pass...  102 us
    pallas_call x1, Pallas kernels, settle(): pl.pallas_call(settle_kernel, out_shape=tuple((jax.ShapeDtypeStruct(a.sha...  2.63 us

profile of v6, /device:TPU:1, one launch (start us, length us, event | category | flops | bytes accessed | tf_op | source)
XLA Modules:
  0.0 105.1 jit_solution(8503018307136260533)
XLA Ops:
  0.6 101.9 %shard_map.112 = (bf16[256,2048]{1,0:T(8,128)(2,1)}, bf16[256,2048]{1,0:T(8,128)(2,1)}, f32[512,256]{1,0:T(8,128)}) custom-call(s32[4,8]{1,0:T(4,128)} %bitcast.4, bf16[1024,512]{1,0:T(8,128)(2,1)} %bitcast.3, bf16[1024,256]{1,0:T(8,128)(2,1)} %q_hbm.1, bf16[1024,256]{1,0:T(8,128)(2,1)} %g_hbm.1, bf16[2048,256]{1,0:T(8,128)(2,1)} %wq_hbm.1, ...), custom_call_target="tpu_custom_call" | custom-call | tf_op jit(solution)/shard_map/pallas_call | solution.py:1191
  102.5 2.6 %shard_map.113 = (bf16[256,2048]{1,0:T(8,128)(2,1)}, bf16[256,2048]{1,0:T(8,128)(2,1)}, f32[512,256]{1,0:T(8,128)}) custom-call(bf16[256,2048]{1,0:T(8,128)(2,1)} %get-tuple-element.9.refs_0_, bf16[256,2048]{1,0:T(8,128)(2,1)} %get-tuple-element.10.refs_1_, f32[512,256]{1,0:T(8,128)} %get-tuple-element.11.refs_2_), custom_call_target="tpu_custom_call" | custom-call | tf_op jit(solution)/shard_map/pallas_call | solution.py:1151

commit v7 on v6

--- a/solution.py
+++ b/solution.py
@@ -679,13 +679,14 @@
     def early_step(i, c):
         project(small(i), lambda: own_send(0, i))
 
-        @pl.when(i >= 1)
-        def _():
-            relay(0, 1, i - 1)
+        for d in range(1, st_n):
+            @pl.when(i >= d)
+            def _():
+                relay(0, d, i - d)
 
         @pl.when(edge | (i == 0))
         def _():
-            own_send(1, i, outward=False)
+            own_send(1, i)
 
         gates(i)
         return c
@@ -708,13 +709,17 @@
         own_send(1, i, inward=False)
         return c
 
-    lax.fori_loop(0, n_some, second_step, 0)
-    lax.fori_loop(0, n_some, outward_send, 0)
+    lax.fori_loop(n_some - 2, n_some, second_step, 0)
+    @pl.when(edge)
+    def _():
+        relay(1, 1, 0)
+
+    lax.fori_loop(jnp.where(edge, n_some, 1), n_some, outward_send, 0)
 
     def late_step(i, c):
         project(large(i), lambda: None)
         for q in range(n_part):
-            @pl.when(edge)
+            @pl.when(edge & (i * n_part + q >= n_some - 3))
             def _():
                 relay(0, 3, i * n_part + q)
 
@@ -761,7 +766,7 @@
     relays = (st_n - 1) * n_some
     lax.fori_loop(0, n_some // n_part, late_step, 0)
     w_beside.start()
-    relay_rest(1, 0, jnp.where(edge, n_some, 0))
+    relay_rest(1, 1, jnp.where(edge, n_some, 1))
     landed(wqg, lsem.at[5])
     order_copy.wait()
     twin_wait(0)
@@ -866,43 +871,60 @@
     give_back(2, ks, key_cols, key_peer, 1, st_n)
     keep_own(key_cols)
 
+    @pl.when(jnp.logical_not(edge))
+    def _():
+        give_back(1, vs_all, value_cols, near_peer, st_n - 1, st_n)
+
     n_tile = tile_of(model, 512)
 
-    def expand(h):
+    n_tiles = model // n_tile
+    tok_pair = tok_rows // tp_n
+
+    def tile(i):
+        return pl.ds(pl.multiple_of(i * n_tile, n_tile), n_tile)
+
+    def expand(h, i):
         a = gboth[pl.ds(pl.multiple_of(h * 2 * tok_pair, tok_pair), 2 * tok_pair), :]
-
-        def step(i, c):
-            n = pl.ds(pl.multiple_of(i * n_tile, n_tile), n_tile)
-            part = dot(a, wqg[n, :], NT).astype(BF)
-            tp_part[h * 2, :, n] = part[:tok_pair]
-            tp_part[h * 2 + 1, :, n] = part[tok_pair:]
-            return c
-
-        lax.fori_loop(0, model // n_tile, step, 0)
-
-    def pair_copy(h):
-        return remote(tp_part.at[h * 2 + 1 - lo], tp_pair.at[h], ps.at[0], pr.at[h], mate)
-
-    def cross(h):
-        return remote(
-            tp_part.at[h * 2 + lo], tp_recv.at[hi], xs.at[0], xr.at[0], {"tp": h * 2 + lo}
-        )
+        part = dot(a, wqg[tile(i), :], NT).astype(BF)
+        tp_part[h * 2, :, tile(i)] = part[:tok_pair]
+        tp_part[h * 2 + 1, :, tile(i)] = part[tok_pair:]
+
+    def pair_copy(h, n, slot):
+        src, dst = tp_part.at[h * 2 + 1 - lo, :, n], tp_pair.at[h, :, n]
+        return remote(src, dst, ps.at[0], pr.at[slot], mate)
+
+    def cross(h, n):
+        src, dst = tp_part.at[h * 2 + lo, :, n], tp_recv.at[hi, :, n]
+        return remote(src, dst, xs.at[0], xr.at[0], {"tp": h * 2 + lo})
 
     for d in range(1, hi_n):
         w_wait(0, ((hi + d) % hi_n) * 2 + lo, w_mine)
         w_twin(d).start()
         w_onward(d, 0).start()
 
-    tok_pair = tok_rows // tp_n
-    for d in range(1, hi_n + 1):
-        h = (hi + d) % hi_n
-        expand(h)
-        pair_copy(h).start()
-    for d in range(1, hi_n):
-        h = (hi + d) % hi_n
-        pair_copy(h).wait_recv()
-        tp_part[h * 2 + lo] = (tp_part[h * 2 + lo].astype(F32) + tp_pair[h].astype(F32)).astype(BF)
-        cross(h).start()
+    there = 1 - hi
+
+    def far_tile(i, c):
+        expand(there, i)
+        pair_copy(there, tile(i), 1 + i).start()
+        return c
+
+    def cross_tile(i, c):
+        n = tile(i)
+        pair_copy(there, n, 1 + i).wait_recv()
+        own = tp_part[there * 2 + lo, :, n].astype(F32)
+        tp_part[there * 2 + lo, :, n] = (own + tp_pair[there, :, n].astype(F32)).astype(BF)
+        cross(there, n).start()
+        return c
+
+    def own_tile(i, c):
+        expand(hi, i)
+        return c
+
+    lax.fori_loop(0, n_tiles, far_tile, 0)
+    lax.fori_loop(0, n_tiles, cross_tile, 0)
+    lax.fori_loop(0, n_tiles, own_tile, 0)
+    pair_copy(hi, pl.ds(0, model), 0).start()
 
     def ask_wait(d, c):
         peer = (st + d) % st_n
@@ -922,11 +944,15 @@
 
     lax.fori_loop(0, st_n, hot_step, 0)
 
-    def gather_sums(kind, o, span, first):
+    def gather_sums(kind, o, span, first=False, last=False):
         def step(i, c):
             r = pl.ds(pl.multiple_of(i * m_tile, m_tile), m_tile)
             part = dot(hot[o, r, :], arr[o, :, :, span].reshape(hot_cols, cols))
-            acc[kind, r, :] = part if first else acc[kind, r, :] + part
+            part = part if first else acc[kind, r, :] + part
+            if last:
+                plow[r, span] = part.astype(BF)
+            else:
+                acc[kind, r, :] = part
             return c
 
         lax.fori_loop(0, pass_rows // m_tile, step, 0)
@@ -941,14 +967,13 @@
     def sums_of(part):
         return sums.at[pl.ds(0, tp_n - 1), :, part]
 
-    def grads_of(kind, peer):
+    def grads_of(kind, peer, last=False):
         phase, part, span = (2, ks, key_cols) if kind == 0 else (1, vs_all, value_cols)
         z_wait(phase, half(ret, peer, part), half(arr, peer, part), peer)
-        gather_sums(kind, peer, span, False)
+        gather_sums(kind, peer, span, last=last)
 
     def sums_send(kind):
         part, span = (ks, key_cols) if kind == 0 else (vs_all, value_cols)
-        plow[:, span] = acc[kind].astype(BF)
         for d in range(1, tp_n):
             sums_copy(kind, part, d).start()
         sums[tp, :, span] = plow[pl.ds(pl.multiple_of(tp * sto_pair, sto_pair), sto_pair), span]
@@ -958,19 +983,15 @@
     beside_st = st + 1 - 2 * (st % 2)
     outer = edge
     inner = jnp.logical_not(outer)
-    gather_sums(1, st, value_cols, True)
-    gather_sums(0, st, key_cols, True)
+    gather_sums(1, st, value_cols, first=True)
+    gather_sums(0, st, key_cols, first=True)
     grads_of(1, beside_st)
     grads_of(1, jnp.where(outer, beyond, middle))
 
     grads_of(0, middle)
 
-    @pl.when(inner)
-    def _():
-        give_back(1, vs_all, value_cols, near_peer, st_n - 1, st_n)
-
     grads_of(0, beyond)
-    grads_of(0, beside_st)
+    grads_of(0, beside_st, last=True)
     sums_send(0)
 
     share = model // st_n
@@ -1058,19 +1079,15 @@
     def keep_store(n, part):
         store_out[:, n] = (terms[:, n] + part).astype(BF)
 
-    grads_of(1, jnp.where(outer, middle, beyond))
+    grads_of(1, jnp.where(outer, middle, beyond), last=True)
     sums_send(1)
 
     landed(sums_of(ks), sr.at[0])
     store_terms(key_cols, keep_terms)
 
-    pair_copy(hi).wait_recv()
-    for d in range(1, hi_n):
-        h = (hi + d) % hi_n
-        landed(tp_recv.at[h], xr.at[0])
-    total = tp_part[tp].astype(F32) + tp_pair[hi].astype(F32)
-    for d in range(1, hi_n):
-        total = total + tp_recv[(hi + d) % hi_n].astype(F32)
+    pair_copy(hi, pl.ds(0, model), 0).wait_recv()
+    landed(tp_recv.at[there], xr.at[0])
+    total = tp_part[tp].astype(F32) + tp_pair[hi].astype(F32) + tp_recv[there].astype(F32)
     tok_out[...] = total.astype(BF)
     tok_done = local(2, tok_out, tok_hbm)
 
@@ -1242,7 +1259,7 @@
                 DMA((3,)),
                 DMA((3, st_n - 1)),
                 DMA((1,)),
-                DMA((hi_n,)),
+                DMA((1 + model // tile_of(model, 512),)),
                 DMA((1,)),
                 DMA((1,)),
                 DMA((1,)),

time: 105 us -> 102 us (0.971)
  Pallas kernels: 104 us -> 101 us
    pallas_call x1, Pallas kernels: 102 us -> 98.8 us  [local(): pl.pallas_call(functools.partial(gathered_kernel, st_n, tp_n, depth, pass...]
where the time goes in v7:
time: 102 us
  Pallas kernels  101 us (99%)
    pallas_call x1, Pallas kernels, local(): pl.pallas_call(functools.partial(gathered_kernel, st_n, tp_n, depth, pass...  98.8 us
    pallas_call x1, Pallas kernels, settle(): pl.pallas_call(settle_kernel, out_shape=tuple((jax.ShapeDtypeStruct(a.sha...  2.63 us

profile of v7, /device:TPU:1, one launch (start us, length us, event | category | flops | bytes accessed | tf_op | source)
XLA Modules:
  0.0 102.1 jit_solution(6872755759369315342)
XLA Ops:
  0.6 98.8 %shard_map.112 = (bf16[256,2048]{1,0:T(8,128)(2,1)}, bf16[256,2048]{1,0:T(8,128)(2,1)}, f32[512,256]{1,0:T(8,128)}) custom-call(s32[4,8]{1,0:T(4,128)} %bitcast.4, bf16[1024,512]{1,0:T(8,128)(2,1)} %bitcast.3, bf16[1024,256]{1,0:T(8,128)(2,1)} %q_hbm.1, bf16[1024,256]{1,0:T(8,128)(2,1)} %g_hbm.1, bf16[2048,256]{1,0:T(8,128)(2,1)} %wq_hbm.1, ...), custom_call_target="tpu_custom_call" | custom-call | tf_op jit(solution)/shard_map/pallas_call | solution.py:1208
  99.5 2.6 %shard_map.113 = (bf16[256,2048]{1,0:T(8,128)(2,1)}, bf16[256,2048]{1,0:T(8,128)(2,1)}, f32[512,256]{1,0:T(8,128)}) custom-call(bf16[256,2048]{1,0:T(8,128)(2,1)} %get-tuple-element.9.refs_0_, bf16[256,2048]{1,0:T(8,128)(2,1)} %get-tuple-element.10.refs_1_, f32[512,256]{1,0:T(8,128)} %get-tuple-element.11.refs_2_), custom_call_target="tpu_custom_call" | custom-call | tf_op jit(solution)/shard_map/pallas_call | solution.py:1168

commit v8 on v7

--- a/solution.py
+++ b/solution.py
@@ -719,10 +719,6 @@
     def late_step(i, c):
         project(large(i), lambda: None)
         for q in range(n_part):
-            @pl.when(edge & (i * n_part + q >= n_some - 3))
-            def _():
-                relay(0, 3, i * n_part + q)
-
             @pl.when(jnp.logical_not(edge))
             def _():
                 relay(1, 1, i * n_part + q)
@@ -764,6 +760,7 @@
         lax.fori_loop(first, last, step, 0)
 
     relays = (st_n - 1) * n_some
+    relay_rest(0, 3 * n_some - 3, jnp.where(edge, 3 * n_some, 0))
     lax.fori_loop(0, n_some // n_part, late_step, 0)
     w_beside.start()
     relay_rest(1, 1, jnp.where(edge, n_some, 1))
@@ -934,6 +931,7 @@
     lax.fori_loop(1, st_n, ask_wait, 0)
     hot_cols = depth * pass_len
     m_tile = tile_of(pass_rows, 256)
+    s_tile = tile_of(pass_rows, 1024)
 
     def hot_step(o, c):
         target = ask_in[o][0:1, :hot_cols]
@@ -946,7 +944,7 @@
 
     def gather_sums(kind, o, span, first=False, last=False):
         def step(i, c):
-            r = pl.ds(pl.multiple_of(i * m_tile, m_tile), m_tile)
+            r = pl.ds(pl.multiple_of(i * s_tile, s_tile), s_tile)
             part = dot(hot[o, r, :], arr[o, :, :, span].reshape(hot_cols, cols))
             part = part if first else acc[kind, r, :] + part
             if last:
@@ -955,17 +953,18 @@
                 acc[kind, r, :] = part
             return c
 
-        lax.fori_loop(0, pass_rows // m_tile, step, 0)
+        lax.fori_loop(0, pass_rows // s_tile, step, 0)
 
     sto_pair = pass_rows // tp_n
 
-    def sums_copy(kind, part, d):
-        t = (tp + d) % tp_n
+    far_tps = (there * 2, there * 2 + 1)
+
+    def sums_copy(kind, part, t, far):
         src = plow.at[pl.ds(pl.multiple_of(t * sto_pair, sto_pair), sto_pair), part]
-        return remote(src, sums.at[tp, :, part], ss.at[kind], sr.at[kind], {"tp": t})
-
-    def sums_of(part):
-        return sums.at[pl.ds(0, tp_n - 1), :, part]
+        return remote(src, sums.at[tp, :, part], ss.at[kind], sr.at[kind, far], {"tp": t})
+
+    def sums_of(part, count):
+        return sums.at[pl.ds(0, count), :, part]
 
     def grads_of(kind, peer, last=False):
         phase, part, span = (2, ks, key_cols) if kind == 0 else (1, vs_all, value_cols)
@@ -974,8 +973,9 @@
 
     def sums_send(kind):
         part, span = (ks, key_cols) if kind == 0 else (vs_all, value_cols)
-        for d in range(1, tp_n):
-            sums_copy(kind, part, d).start()
+        for t in far_tps:
+            sums_copy(kind, part, t, 1).start()
+        sums_copy(kind, part, mate_t, 0).start()
         sums[tp, :, span] = plow[pl.ds(pl.multiple_of(tp * sto_pair, sto_pair), sto_pair), span]
 
     beyond = jnp.where(lower, st_n - 1, 0)
@@ -1062,28 +1062,34 @@
         w_onward(d, 1).start()
     landed(wall.at[pl.ds(0, hi_n)], wr.at[2])
 
-    def store_terms(span, done):
+    def store_terms(sources, span, done):
         def step(i, c):
-            n = pl.ds(pl.multiple_of(i * n_tile, n_tile), n_tile)
-            part = dot(sums[0, :, span], wall[0, n, span], NT)
-            for t in range(1, tp_n):
-                part = part + dot(sums[t, :, span], wall[t, n, span], NT)
-            done(n, part)
+            n = tile(i)
+            parts = [dot(sums[t, :, span], wall[t, n, span], NT) for t in sources]
+            done(n, sum(parts[1:], parts[0]))
             return c
 
-        lax.fori_loop(0, model // n_tile, step, 0)
-
-    def keep_terms(n, part):
+        lax.fori_loop(0, n_tiles, step, 0)
+
+    def set_terms(n, part):
         terms[:, n] = part
+
+    def add_terms(n, part):
+        terms[:, n] += part
+
+    def store_tile(n):
+        return pltpu.make_async_copy(store_out.at[:, n], store_hbm.at[:, n], lsem.at[3])
 
     def keep_store(n, part):
         store_out[:, n] = (terms[:, n] + part).astype(BF)
+        store_tile(n).start()
 
     grads_of(1, jnp.where(outer, middle, beyond), last=True)
     sums_send(1)
 
-    landed(sums_of(ks), sr.at[0])
-    store_terms(key_cols, keep_terms)
+    landed(sums_of(ks, 1), sr.at[0, 0])
+    landed(sums_of(ks, 2), sr.at[0, 1])
+    store_terms((tp, mate_t) + far_tps, key_cols, set_terms)
 
     pair_copy(hi, pl.ds(0, model), 0).wait_recv()
     landed(tp_recv.at[there], xr.at[0])
@@ -1095,9 +1101,10 @@
     def _():
         dw_relay(1)
 
-    landed(sums_of(vs_all), sr.at[1])
-    store_terms(value_cols, keep_store)
-    store_done = local(3, store_out, store_hbm)
+    landed(sums_of(vs_all, 1), sr.at[1, 0])
+    store_terms((tp, mate_t), value_cols, add_terms)
+    landed(sums_of(vs_all, 2), sr.at[1, 1])
+    store_terms(far_tps, value_cols, keep_store)
 
     for b in range(bits):
         line = slice(b * bit, (b + 1) * bit)
@@ -1129,12 +1136,12 @@
     sent(ask_in.at[pl.ds(0, st_n - 1)], zs.at[0])
     sent(ret.at[pl.ds(0, st_n - 1), :, :, vs_all], zs.at[1])
     sent(ret.at[pl.ds(0, st_n - 1), :, :, ks], zs.at[2])
-    sent(sums_of(ks), ss.at[0])
-    sent(sums_of(vs_all), ss.at[1])
+    sent(sums_of(ks, tp_n - 1), ss.at[0])
+    sent(sums_of(vs_all, tp_n - 1), ss.at[1])
     sent(tp_pair, ps.at[0])
     sent(tp_recv.at[0], xs.at[0])
     sent(dwp.at[pl.ds(0, 3 * share)], us.at[0])
-    for copy in (tok_done, store_done, wkey_done):
+    for copy in (tok_done, store_tile(pl.ds(0, model)), wkey_done):
         copy.wait()
 
 
@@ -1265,7 +1272,7 @@
                 DMA((1,)),
                 DMA((3,)),
                 DMA((2,)),
-                DMA((2,)),
+                DMA((2, 2)),
                 DMA((1,)),
                 DMA((4, 2)),
             ],

time: 102 us -> 102 us (level)
  no operation moved by 1% of the time
where the time goes in v8:
time: 102 us; the launch traced here: 101 us
  Pallas kernels  101 us (99%)
    pallas_call x1, Pallas kernels, local(): pl.pallas_call(functools.partial(gathered_kernel, st_n, tp_n, depth, pass...  98.1 us
    pallas_call x1, Pallas kernels, settle(): pl.pallas_call(settle_kernel, out_shape=tuple((jax.ShapeDtypeStruct(a.sha...  2.63 us

profile of v8, /device:TPU:1, one launch (start us, length us, event | category | flops | bytes accessed | tf_op | source)
XLA Modules:
  0.0 101.3 jit_solution(5297244746759278534)
XLA Ops:
  0.6 98.1 %shard_map.112 = (bf16[256,2048]{1,0:T(8,128)(2,1)}, bf16[256,2048]{1,0:T(8,128)(2,1)}, f32[512,256]{1,0:T(8,128)}) custom-call(s32[4,8]{1,0:T(4,128)} %bitcast.4, bf16[1024,512]{1,0:T(8,128)(2,1)} %bitcast.3, bf16[1024,256]{1,0:T(8,128)(2,1)} %q_hbm.1, bf16[1024,256]{1,0:T(8,128)(2,1)} %g_hbm.1, bf16[2048,256]{1,0:T(8,128)(2,1)} %wq_hbm.1, ...), custom_call_target="tpu_custom_call" | custom-call | tf_op jit(solution)/shard_map/pallas_call | solution.py:1215
  98.7 2.6 %shard_map.113 = (bf16[256,2048]{1,0:T(8,128)(2,1)}, bf16[256,2048]{1,0:T(8,128)(2,1)}, f32[512,256]{1,0:T(8,128)}) custom-call(bf16[256,2048]{1,0:T(8,128)(2,1)} %get-tuple-element.9.refs_0_, bf16[256,2048]{1,0:T(8,128)(2,1)} %get-tuple-element.10.refs_1_, f32[512,256]{1,0:T(8,128)} %get-tuple-element.11.refs_2_), custom_call_target="tpu_custom_call" | custom-call | tf_op jit(solution)/shard_map/pallas_call | solution.py:1175

commit v9 on v8

--- a/solution.py
+++ b/solution.py
@@ -431,7 +431,7 @@
     st_n, tp_n, depth, pass_len,
     ids_hbm, store_ref, q_hbm, g_hbm, wq_hbm, wg_hbm, wk_hbm, wv_hbm, m_hbm,
     tok_hbm, store_hbm, wkey_hbm,
-    ids_ref, tok_out, store_out, wkey_out, rows, wall, wqg, q_v, g_v, m_v, acc, terms, k_all, v_all, ask_v, ask_in, order_v, req_ref, gated, slope, ret, prob_v, kvb, reqg, gboth, arr,
+    ids_ref, tok_out, store_out, wkey_out, rows, wall, wqg, q_v, g_v, m_v, acc, terms, k_all, v_all, ask_v, ask_in, order_v, req_ref, gated, slope, ret, prob_v, score_v, kvb, reqg, gboth, arr,
     hot, plow, sums, dwp, dwc, dwf, tp_part, tp_pair, tp_recv,
     lsem, gs, gr, fs, fr, fw, zs, zr, ps, pr, xs, xr, ws, wr, ss, sr, us, ur,
 ):
@@ -840,7 +840,6 @@
 
     def block_step(i, c):
         for n in pairs:
-            fill(n, k_all, key_cols, 4 * i + n)
             fill(n, v_all, value_cols, 4 * i + n)
         for head in range(heads):
             hs = slice(head * HD, (head + 1) * HD)
@@ -848,16 +847,27 @@
             for n in pairs:
                 b = 4 * i + n
                 r = block_rows(b)
-                value = kvb[n, :, vs]
                 prob = prob_v[head, r, :]
-                prob_grad = dot(gated[r, hs], value, NT)
+                prob_grad = dot(gated[r, hs], kvb[n, :, vs], NT)
                 inner = jnp.sum(prob * prob_grad, axis=-1, keepdims=True)
                 score_grad = (scale * prob * (prob_grad - inner)).astype(BF)
+                score_v[head, r, :] = score_grad
                 key_grad = dot(score_grad, q_v[r, hs], TN).astype(BF)
                 for j in range(PB):
                     reqg[j * blocks + b, :, hs] = key_grad[j * pass_len : (j + 1) * pass_len]
-                gboth[r, hs] = dot(score_grad, kvb[n, :, hs]).astype(BF)
-                attended = dot(prob.astype(BF), value)
+        return c
+
+    def token_step(i, c):
+        for n in pairs:
+            fill(n, k_all, key_cols, 4 * i + n)
+            fill(n, v_all, value_cols, 4 * i + n)
+        for head in range(heads):
+            hs = slice(head * HD, (head + 1) * HD)
+            vs = slice(cols + head * HD, cols + (head + 1) * HD)
+            for n in pairs:
+                r = block_rows(4 * i + n)
+                gboth[r, hs] = dot(score_v[head, r, :], kvb[n, :, hs]).astype(BF)
+                attended = dot(prob_v[head, r, :].astype(BF), kvb[n, :, vs])
                 gboth[r, vs] = (attended * slope[r, hs]).astype(BF)
         return c
 
@@ -894,17 +904,17 @@
         src, dst = tp_part.at[h * 2 + lo, :, n], tp_recv.at[hi, :, n]
         return remote(src, dst, xs.at[0], xr.at[0], {"tp": h * 2 + lo})
 
+    there = 1 - hi
+
+    def far_tile(i, c):
+        expand(there, i)
+        pair_copy(there, tile(i), 1 + i).start()
+        return c
+
     for d in range(1, hi_n):
         w_wait(0, ((hi + d) % hi_n) * 2 + lo, w_mine)
         w_twin(d).start()
         w_onward(d, 0).start()
-
-    there = 1 - hi
-
-    def far_tile(i, c):
-        expand(there, i)
-        pair_copy(there, tile(i), 1 + i).start()
-        return c
 
     def cross_tile(i, c):
         n = tile(i)
@@ -918,7 +928,9 @@
         expand(hi, i)
         return c
 
+    token_step(there, 0)
     lax.fori_loop(0, n_tiles, far_tile, 0)
+    token_step(hi, 0)
     lax.fori_loop(0, n_tiles, cross_tile, 0)
     lax.fori_loop(0, n_tiles, own_tile, 0)
     pair_copy(hi, pl.ds(0, model), 0).start()
@@ -1208,7 +1220,7 @@
     gathered_bytes = 2 * 2 * st_n * pass_rows * cols
     steps = blocks // 4
     fits = lax.axis_size("grp") == 2 and hi_n == 2 and st_n == 4 and st_n == tp_n
-    fits = fits and passages % 4 == 0 and blocks % 4 == 0 and passages // 4 % steps == 0
+    fits = fits and passages % 4 == 0 and blocks % 4 == 0 and steps == hi_n and passages // 4 % steps == 0
     if fits and gathered_bytes <= 8 << 20:
         half_pass = passages // 2
         n_some = half_pass // tile_of(half_pass, 2)
@@ -1244,6 +1256,7 @@
                 V((tok_rows, cols), F32),
                 V((st_n, depth, pass_len, pair), BF),
                 V((cols // HD, tok_rows, PB * pass_len), F32),
+                V((cols // HD, tok_rows, PB * pass_len), BF),
                 V((4, PB * pass_len, pair), BF),
                 V((requests, pass_len, pair), BF),
                 V((tok_rows, pair), BF),

time: 102 us -> 101 us (level)
  no operation moved by 1% of the time
where the time goes in v9:
time: 101 us
  Pallas kernels  100 us (99%)
    pallas_call x1, Pallas kernels, local(): pl.pallas_call(functools.partial(gathered_kernel, st_n, tp_n, depth, pass...  97.4 us
    pallas_call x1, Pallas kernels, settle(): pl.pallas_call(settle_kernel, out_shape=tuple((jax.ShapeDtypeStruct(a.sha...  2.63 us

profile of v9, /device:TPU:1, one launch (start us, length us, event | category | flops | bytes accessed | tf_op | source)
XLA Modules:
  0.0 100.7 jit_solution(14793588716160735943)
XLA Ops:
  0.6 97.4 %shard_map.112 = (bf16[256,2048]{1,0:T(8,128)(2,1)}, bf16[256,2048]{1,0:T(8,128)(2,1)}, f32[512,256]{1,0:T(8,128)}) custom-call(s32[4,8]{1,0:T(4,128)} %bitcast.4, bf16[1024,512]{1,0:T(8,128)(2,1)} %bitcast.3, bf16[1024,256]{1,0:T(8,128)(2,1)} %q_hbm.1, bf16[1024,256]{1,0:T(8,128)(2,1)} %g_hbm.1, bf16[2048,256]{1,0:T(8,128)(2,1)} %wq_hbm.1, ...), custom_call_target="tpu_custom_call" | custom-call | tf_op jit(solution)/shard_map/pallas_call | solution.py:1227
  98.0 2.6 %shard_map.113 = (bf16[256,2048]{1,0:T(8,128)(2,1)}, bf16[256,2048]{1,0:T(8,128)(2,1)}, f32[512,256]{1,0:T(8,128)}) custom-call(bf16[256,2048]{1,0:T(8,128)(2,1)} %get-tuple-element.9.refs_0_, bf16[256,2048]{1,0:T(8,128)(2,1)} %get-tuple-element.10.refs_1_, f32[512,256]{1,0:T(8,128)} %get-tuple-element.11.refs_2_), custom_call_target="tpu_custom_call" | custom-call | tf_op jit(solution)/shard_map/pallas_call | solution.py:1187

commit v10 on v9

--- a/solution.py
+++ b/solution.py
@@ -930,8 +930,8 @@
 
     token_step(there, 0)
     lax.fori_loop(0, n_tiles, far_tile, 0)
+    lax.fori_loop(0, n_tiles, cross_tile, 0)
     token_step(hi, 0)
-    lax.fori_loop(0, n_tiles, cross_tile, 0)
     lax.fori_loop(0, n_tiles, own_tile, 0)
     pair_copy(hi, pl.ds(0, model), 0).start()
 

time: 101 us -> 101 us (level)
  no operation moved by 1% of the time
where the time goes in v10:
time: 101 us
  Pallas kernels  99.9 us (99%)
    pallas_call x1, Pallas kernels, local(): pl.pallas_call(functools.partial(gathered_kernel, st_n, tp_n, depth, pass...  97.3 us
    pallas_call x1, Pallas kernels, settle(): pl.pallas_call(settle_kernel, out_shape=tuple((jax.ShapeDtypeStruct(a.sha...  2.63 us

profile of v10, /device:TPU:1, one launch (start us, length us, event | category | flops | bytes accessed | tf_op | source)
XLA Modules:
  0.0 100.5 jit_solution(1681569709628492992)
XLA Ops:
  0.6 97.3 %shard_map.112 = (bf16[256,2048]{1,0:T(8,128)(2,1)}, bf16[256,2048]{1,0:T(8,128)(2,1)}, f32[512,256]{1,0:T(8,128)}) custom-call(s32[4,8]{1,0:T(4,128)} %bitcast.4, bf16[1024,512]{1,0:T(8,128)(2,1)} %bitcast.3, bf16[1024,256]{1,0:T(8,128)(2,1)} %q_hbm.1, bf16[1024,256]{1,0:T(8,128)(2,1)} %g_hbm.1, bf16[2048,256]{1,0:T(8,128)(2,1)} %wq_hbm.1, ...), custom_call_target="tpu_custom_call" | custom-call | tf_op jit(solution)/shard_map/pallas_call | solution.py:1227
  97.9 2.6 %shard_map.113 = (bf16[256,2048]{1,0:T(8,128)(2,1)}, bf16[256,2048]{1,0:T(8,128)(2,1)}, f32[512,256]{1,0:T(8,128)}) custom-call(bf16[256,2048]{1,0:T(8,128)(2,1)} %get-tuple-element.9.refs_0_, bf16[256,2048]{1,0:T(8,128)(2,1)} %get-tuple-element.10.refs_1_, f32[512,256]{1,0:T(8,128)} %get-tuple-element.11.refs_2_), custom_call_target="tpu_custom_call" | custom-call | tf_op jit(solution)/shard_map/pallas_call | solution.py:1187
